TPU v7x, 128 devices: a whole 4x4x4 slice. The times are simulated.
128 devices in a mesh: rep: 2 (over z_hi), fs: 32 (over z_lo, y, x), tp: 2 (over core).
Axes of the slice: x: 4, y: 4, z: 4 (z_hi: 2, z_lo: 2; z = z_hi * 2 + z_lo), core: 2. Of those that a mesh axis runs over, the one named last changes fastest.
Arguments:
- later_input: bfloat16 [32768, 2048], P(('rep', 'fs', 'tp')), may hold values from -6 to 6
- earlier_input: bfloat16 [32768, 2048], P(('rep', 'fs', 'tp')), may hold values from -6 to 6
- hidden_cot: bfloat16 [32768, 2816], P(('rep', 'fs'), 'tp'), may hold values from -8 to 8
- norm_gain: float32 [2048], replicated, may hold values from 0.1 to 1.9
- gate_weight: bfloat16 [2048, 2816], P('fs', 'tp'), may hold values from -0.125 to 0.125
- up_weight: bfloat16 [2048, 2816], P('fs', 'tp'), may hold values from -0.125 to 0.125
- gate_running: float32 [2048, 2816], P('fs', 'tp'), may hold values from -6 to 6
- up_running: float32 [2048, 2816], P('fs', 'tp'), may hold values from -6 to 6
- gain_running: float32 [2048], replicated, may hold values from -6 to 6
Outputs:
- later_hidden: bfloat16 [32768, 2816], P(('rep', 'fs'), 'tp')
- earlier_grad: bfloat16 [32768, 2048], P(('rep', 'fs', 'tp'))
- gate_total: float32 [2048, 2816], P('fs', 'tp')
- up_total: float32 [2048, 2816], P('fs', 'tp')
- gain_total: float32 [2048], replicated
All inputs are finite; a program needn't handle non-finite values.
Results may differ from a plain program's by a relative error of at most 0.015.
Values may be sent and summed in bfloat16 or wider, within the bound.
A program may use at most 128 MiB of HBM per device.

v0:
```python
import math

import jax
import jax.numpy as jnp
from jax import lax
from jax.sharding import PartitionSpec as P

EPSILON = 1e-06
CONTRACT_ROWS = (((0,), (0,)), ((), ()))
CONTRACT_COLS = (((1,), (1,)), ((), ()))


def in_one_piece(arrays, axis, dim, along):
    ends, at = ([], 0)
    for a in arrays[:-1]:
        at += a.shape[along]
        ends.append(at)
    both = jnp.concatenate(arrays, axis=along)
    return tuple(jnp.split(lax.all_gather(both, axis, axis=dim, tiled=True), ends, axis=along))


def sent_to_all(array, axis):
    peers = lax.axis_size(axis)
    return lax.all_to_all(
        jnp.broadcast_to(array[None], (peers, *array.shape)), axis, 0, 0, tiled=True
    )


def over_copies(array, axis):
    return sent_to_all(array, axis).astype(jnp.float32).sum(axis=0)


def normalize(activation, norm_gain):
    values = activation.astype(jnp.float32)
    inv_rms = lax.rsqrt(jnp.mean(values * values, axis=1, keepdims=True) + EPSILON)
    return (values, inv_rms, (values * inv_rms * norm_gain).astype(jnp.bfloat16))


def make_term(source, d_gate, d_up):
    gate_part = lax.dot_general(source, d_gate, CONTRACT_ROWS, preferred_element_type=jnp.float32)
    up_part = lax.dot_general(source, d_up, CONTRACT_ROWS, preferred_element_type=jnp.float32)
    return jnp.concatenate([gate_part, up_part], axis=1)


def body(
    later_input,
    earlier_input,
    hidden_cot,
    norm_gain,
    gate_weight,
    up_weight,
    gate_running,
    up_running,
    gain_running,
):
    local_rows = later_input.shape[0]
    width_tp = gate_weight.shape[1]
    count_rep = lax.axis_size("rep")
    count_fs = lax.axis_size("fs")
    count_tp = lax.axis_size("tp")
    factor = 1.0 / math.sqrt(local_rows * count_rep * count_fs * count_tp)
    later_vals, later_inv, later_norm = normalize(later_input, norm_gain)
    earlier_vals, earlier_inv, earlier_norm = normalize(earlier_input, norm_gain)
    later_rows, earlier_rows = (
        lax.all_gather(later_norm, "tp", axis=0, tiled=True),
        lax.all_gather(earlier_norm, "tp", axis=0, tiled=True),
    )
    gate_whole, up_whole = in_one_piece((gate_weight, up_weight), "fs", 0, 1)
    later_gate = jnp.dot(later_rows, gate_whole, preferred_element_type=jnp.float32)
    later_up = jnp.dot(later_rows, up_whole, preferred_element_type=jnp.float32)
    later_hidden = (jax.nn.silu(later_gate) * later_up).astype(jnp.bfloat16)
    earlier_gate = jnp.dot(earlier_rows, gate_whole, preferred_element_type=jnp.float32)
    earlier_up = jnp.dot(earlier_rows, up_whole, preferred_element_type=jnp.float32)
    gate_sigmoid = jax.nn.sigmoid(earlier_gate)
    upstream = hidden_cot.astype(jnp.float32)
    d_up = (upstream * earlier_gate * gate_sigmoid).astype(jnp.bfloat16)
    d_gate = (
        upstream * earlier_up * gate_sigmoid * (1.0 + earlier_gate * (1.0 - gate_sigmoid))
    ).astype(jnp.bfloat16)
    result = lax.dot_general(d_gate, gate_whole, CONTRACT_COLS, preferred_element_type=jnp.float32)
    d_norm = lax.psum_scatter(
        (
            result
            + lax.dot_general(d_up, up_whole, CONTRACT_COLS, preferred_element_type=jnp.float32)
        ).astype(jnp.bfloat16),
        "tp",
        scatter_dimension=0,
        tiled=True,
    ).astype(jnp.float32)
    scaled = d_norm * norm_gain
    inner = jnp.mean(scaled * earlier_vals, axis=1, keepdims=True)
    earlier_grad = (earlier_inv * scaled - earlier_vals * earlier_inv**3 * inner).astype(
        jnp.bfloat16
    )
    gain_local = jnp.sum(d_norm * earlier_vals * earlier_inv, axis=0)
    gain_sum = lax.psum(gain_local, ("rep", "fs", "tp"))
    own_part = lax.psum_scatter(
        make_term(earlier_rows, d_gate, d_up).astype(jnp.bfloat16),
        "fs",
        scatter_dimension=0,
        tiled=True,
    )
    summed = over_copies(own_part, "rep").astype(jnp.float32)
    gate_total = gate_running + factor * summed[:, :width_tp]
    up_total = up_running + factor * summed[:, width_tp:]
    gain_total = gain_running + factor * gain_sum
    return (later_hidden, earlier_grad, gate_total, up_total, gain_total)


def solution(mesh):
    in_specs = (
        P(("rep", "fs", "tp"), None),
        P(("rep", "fs", "tp"), None),
        P(("rep", "fs"), "tp"),
        P(),
        P("fs", "tp"),
        P("fs", "tp"),
        P("fs", "tp"),
        P("fs", "tp"),
        P(),
    )
    out_specs = (
        P(("rep", "fs"), "tp"),
        P(("rep", "fs", "tp"), None),
        P("fs", "tp"),
        P("fs", "tp"),
        P(),
    )
    return jax.shard_map(body, mesh=mesh, in_specs=in_specs, out_specs=out_specs, check_vma=False)
```

profile of v0, /device:TPU:0, one launch (start us, length us, event | category | flops | bytes accessed | tf_op | source)
XLA Modules:
  0.0 491.1 jit_solution(415019775626761641)
XLA Ops:
  7.2 0.0 copy-start.4
  7.2 0.0 copy-start.5
  7.2 0.0 all-gather.8.cloned.1.call-start
  7.2 1.6 fusion.39
  8.8 2.5 fusion.41
  11.4 0.0 all-gather.8.cloned.1.call-update
  11.4 0.0 all-gather.6.cloned.1.call-start
  11.4 0.8 pad_maximum_fusion.1
  12.2 0.0 all-gather.6.cloned.1.call-update
  12.2 0.0 copy-start.12
  12.2 0.0 reduce-scatter.5.cloned.1.call-start
  12.3 15.0 %all-gather.8.cloned.1.call-done = bf16[512,2048]{1,0:T(8,128)(2,1)} async-done(((bf16[256,2048]{1,0:T(8,128)(2,1)}), bf16[512,2048]{1,0:T(8,128)(2,1)}) %all-gather.8.cloned.1.call-update) | async-done | bytes 2097168 | tf_op jit(solution)/shard_map/all_gather | solution.py:66
  27.3 175.7 %all-gather.6.cloned.1.call-done = bf16[2048,2816]{1,0:T(8,128)(2,1)} async-done(((bf16[64,2816]{1,0:T(8,128)(2,1)}), bf16[2048,2816]{1,0:T(8,128)(2,1)}) %all-gather.6.cloned.1.call-update) | async-done | bytes 11534352 | tf_op jit(solution)/shard_map/all_gather | solution.py:19
  203.0 6.6 %fusion.8 = f32[512,1408]{1,0:T(8,128)S(1)} fusion(bf16[512,2048]{1,0:T(8,128)(2,1)} %all-gather.8.cloned.1.call-done, bf16[2048,2816]{1,0:T(8,128)(2,1)} %all-gather.6.cloned.1.call-done), kind=kOutput, calls=%fused_computation.11 | convolution fusion | flops 2952790016 | bytes 10747904 | tf_op jit(solution)/shard_map/dot_general | solution.py:72
  209.5 0.2 copy-done.8
  209.7 4.0 fusion.25
  213.7 0.0 copy-start.14
  213.7 3.5 fusion
  217.2 0.0 copy-start.1
  217.2 4.7 add_convert_fusion
  221.9 0.0 reduce-scatter.5.cloned.1.call-update
  221.9 0.0 all-gather.4.cloned.1.call-start
  222.0 0.0 copy-done.1
  222.0 0.3 fusion.36
  222.3 10.9 %reduce-scatter.5.cloned.1.call-done = bf16[256,2048]{1,0:T(8,128)(2,1)} async-done(((bf16[512,2048]{1,0:T(8,128)(2,1)}), bf16[256,2048]{1,0:T(8,128)(2,1)}) %reduce-scatter.5.cloned.1.call-update) | async-done | bytes 1048592 | tf_op jit(solution)/shard_map/reduce_scatter | solution.py:81
  233.1 0.0 copy-done.6
  233.1 1.9 fusion.45
  235.0 3.3 fusion.35
  238.4 0.0 all-gather.4.cloned.1.call-update
  238.4 0.0 copy-start.13
  238.4 0.2 reduce-scatter.7.cloned.1.call-start
  238.6 5.3 %convolution_convert_fusion.1 = bf16[2048,1408]{0,1:T(8,128)(2,1)S(1)} fusion(bf16[512,2048]{1,0:T(8,128)(2,1)} %all-gather.8.cloned.1.call-done, bf16[512,1408]{1,0:T(8,128)(2,1)} %copy-done.14), kind=kOutput, calls=%fused_computation.2 | convolution fusion | flops 2955673600 | bytes 9306112 | tf_op jit(solution)/shard_map/dot_general | solution.py:40
  244.0 3.9 convolution_convert_fusion
  247.9 13.8 %pad_maximum_fusion = bf16[2048,2816]{0,1:T(8,128)(2,1)} fusion(bf16[2048,1408]{0,1:T(8,128)(2,1)S(1)} %convolution_convert_fusion, bf16[2048,1408]{0,1:T(8,128)(2,1)S(1)} %convolution_convert_fusion.1), kind=kLoop, calls=%fused_computation | loop fusion | flops 23068672 | bytes 23068672 | tf_op jit(solution)/shard_map/concatenate | solution.py:42
  261.7 15.3 %copy.17 = bf16[2048,2816]{1,0:T(8,128)(2,1)} copy(bf16[2048,2816]{0,1:T(8,128)(2,1)} %pad_maximum_fusion) | data formatting | bytes 23068672
  277.0 0.0 reduce-scatter.7.cloned.1.call-update
  277.1 79.6 %psum.7 = f32[2048]{0:T(1024)S(1)} all-reduce(f32[2048]{0:T(1024)S(1)} %get-tuple-element.5), channel_id=1, replica_groups=mesh['rep'=2,'fs'=32,'tp'=2] {'rep','fs','tp'}, use_global_device_ids=true, to_apply=%region_7.8 | all-reduce | flops 2048 | bytes 16384 | tf_op jit(solution)/shard_map/psum | solution.py:96
  356.7 0.6 multiply_add_fusion
  357.3 8.5 %fusion.10 = f32[512,1408]{1,0:T(8,128)} fusion(bf16[512,2048]{1,0:T(8,128)(2,1)} %all-gather.4.cloned.1.call-done, bf16[2048,2816]{1,0:T(8,128)(2,1)} %all-gather.6.cloned.1.call-done), kind=kOutput, calls=%fused_computation.13 | convolution fusion | flops 2952790016 | bytes 10747904 | tf_op jit(solution)/shard_map/dot_general | solution.py:69
  365.8 101.2 %reduce-scatter.7.cloned.1.call-done = bf16[64,2816]{1,0:T(8,128)(2,1)} async-done(((bf16[2048,2816]{1,0:T(8,128)(2,1)}), bf16[64,2816]{1,0:T(8,128)(2,1)}) %reduce-scatter.7.cloned.1.call-update) | async-done | bytes 360464 | tf_op jit(solution)/shard_map/reduce_scatter | solution.py:97
  467.0 1.9 broadcast_in_dim.2
  468.9 5.5 %all-to-all-start = ((bf16[2,64,2816]{2,1,0:T(8,128)(2,1)}), bf16[2,64,2816]{2,1,0:T(8,128)(2,1)S(1)}, u32[]{:S(2)}, u32[]{:S(2)}) async-start(bf16[2,64,2816]{2,1,0:T(8,128)(2,1)} %broadcast_in_dim.2), calls=%async_computation.1 | async-start | bytes 1441792 | tf_op jit(solution)/shard_map/all_to_all | solution.py:24
  474.4 7.7 %fusion.28 = bf16[512,1408]{1,0:T(8,128)(2,1)} fusion(bf16[512,2048]{1,0:T(8,128)(2,1)S(1)} %copy-done.11, bf16[2048,2816]{1,0:T(8,128)(2,1)} %all-gather.6.cloned.1.call-done, f32[512,1408]{1,0:T(8,128)} %fusion.10), kind=kOutput, calls=%fused_computation.27 | convolution fusion | flops 2957115392 | bytes 12189696 | tf_op jit(solution)/shard_map/dot_general | solution.py:70
  482.1 1.4 all-to-all-done
  483.5 0.1 convert_reduce_fusion
  483.6 0.0 copy-done.2
  483.6 0.0 copy-done.3
  483.6 0.9 fusion.46
  (27 shorter events, 0.1 us)
Async XLA Ops:
  7.2 4.3 copy-start.4
  7.2 4.3 copy-start.5
  7.2 20.1 %all-gather.8.cloned.1.call-start = ((), (), s32[]{:S(2)}) async-start(), calls=%async_computation.5 | async-start | bytes 3145728 | tf_op jit(solution)/shard_map/all_gather | solution.py:66
  11.4 191.6 %all-gather.6.cloned.1.call-start = ((), (), s32[]{:S(2)}) async-start(), calls=%async_computation.4 | async-start | bytes 11894784 | tf_op jit(solution)/shard_map/all_gather | solution.py:19
  12.2 197.3 %copy-start.12 = (bf16[512,1408]{1,0:T(8,128)(2,1)S(1)}, bf16[512,1408]{1,0:T(8,128)(2,1)}, u32[]{:S(2)}) copy-start(bf16[512,1408]{1,0:T(8,128)(2,1)} %param.11) | copy-start | bytes 4325380
  12.2 220.9 %reduce-scatter.5.cloned.1.call-start = ((), (), s32[]{:S(2)}) async-start(), calls=%async_computation.6 | async-start | bytes 3145728 | tf_op jit(solution)/shard_map/reduce_scatter | solution.py:81
  27.3 182.3 %copy-start.9 = (bf16[512,2048]{1,0:T(8,128)(2,1)S(1)}, bf16[512,2048]{1,0:T(8,128)(2,1)}, u32[]{:S(2)}) copy-start(bf16[512,2048]{1,0:T(8,128)(2,1)} %all-gather.8.cloned.1.call-done) | copy-start | bytes 6291460
  203.0 6.8 %copy-start.8 = (bf16[2048,2816]{1,0:T(8,128)(2,1)S(1)}, bf16[2048,2816]{1,0:T(8,128)(2,1)}, u32[]{:S(2)}) copy-start(bf16[2048,2816]{1,0:T(8,128)(2,1)} %all-gather.6.cloned.1.call-done) | copy-start | bytes 34603012
  209.7 4.0 copy-start.15
  213.7 3.5 copy-start.14
  217.2 4.8 copy-start.1
  221.9 11.3 %copy-start = (bf16[256,2048]{1,0:T(8,128)(2,1)S(1)}, bf16[256,2048]{1,0:T(8,128)(2,1)}, u32[]{:S(2)}) copy-start(bf16[256,2048]{1,0:T(8,128)(2,1)} %param.10) | copy-start | bytes 3145732
  221.9 11.3 %copy-start.6 = (f32[2048]{0:T(1024)S(1)}, f32[2048]{0:T(1024)}, u32[]{:S(2)}) copy-start(f32[2048]{0:T(1024)} %param.12) | copy-start | bytes 24580
  221.9 135.4 %all-gather.4.cloned.1.call-start = ((), (), s32[]{:S(2)}) async-start(), calls=%async_computation.3 | async-start | bytes 3145728 | tf_op jit(solution)/shard_map/all_gather | solution.py:65
  238.4 5.6 %copy-start.10 = (bf16[512,2048]{1,0:T(8,128)(2,1)S(1)}, bf16[512,2048]{1,0:T(8,128)(2,1)}, u32[]{:S(2)}) copy-start(bf16[512,2048]{1,0:T(8,128)(2,1)} %all-gather.8.cloned.1.call-done) | copy-start | bytes 6291460
  238.4 5.6 %copy-start.13 = (bf16[512,1408]{1,0:T(8,128)(2,1)S(1)}, bf16[512,1408]{1,0:T(8,128)(2,1)}, u32[]{:S(2)}) copy-start(bf16[512,1408]{1,0:T(8,128)(2,1)} %param.11) | copy-start | bytes 4325380
  238.4 228.6 %reduce-scatter.7.cloned.1.call-start = ((), (), s32[]{:S(2)}) async-start(), calls=%async_computation.7 | async-start | bytes 11894784 | tf_op jit(solution)/shard_map/reduce_scatter | solution.py:97
  238.6 5.4 %copy-start.16 = (f32[512,1408]{1,0:T(8,128)S(1)}, f32[512,1408]{1,0:T(8,128)}, u32[]{:S(2)}) copy-start(f32[512,1408]{1,0:T(8,128)} %copy-done.15) | copy-start | bytes 8650756
  277.0 79.6 %copy-start.7 = (f32[2048]{0:T(1024)S(1)}, f32[2048]{0:T(1024)}, u32[]{:S(2)}) copy-start(f32[2048]{0:T(1024)} %param.17) | copy-start | bytes 24580
  357.3 117.1 %copy-start.11 = (bf16[512,2048]{1,0:T(8,128)(2,1)S(1)}, bf16[512,2048]{1,0:T(8,128)(2,1)}, u32[]{:S(2)}) copy-start(bf16[512,2048]{1,0:T(8,128)(2,1)} %all-gather.4.cloned.1.call-done) | copy-start | bytes 6291460
  468.9 14.6 %all-to-all-start = ((bf16[2,64,2816]{2,1,0:T(8,128)(2,1)}), bf16[2,64,2816]{2,1,0:T(8,128)(2,1)S(1)}, u32[]{:S(2)}, u32[]{:S(2)}) async-start(bf16[2,64,2816]{2,1,0:T(8,128)(2,1)} %broadcast_in_dim.2), calls=%async_computation.1 | async-start | bytes 1441792 | tf_op jit(solution)/shard_map/all_to_all | solution.py:24
  474.4 9.3 %copy-start.2 = (f32[64,1408]{1,0:T(8,128)S(1)}, f32[64,1408]{1,0:T(8,128)}, u32[]{:S(2)}) copy-start(f32[64,1408]{1,0:T(8,128)} %param.16) | copy-start | bytes 1081348
  474.4 9.3 %copy-start.3 = (f32[64,1408]{1,0:T(8,128)S(1)}, f32[64,1408]{1,0:T(8,128)}, u32[]{:S(2)}) copy-start(f32[64,1408]{1,0:T(8,128)} %param.15) | copy-start | bytes 1081348
Sparse Core Ops, SparseCore 0:
  11.5 15.7 all-gather.7
  29.5 173.4 all-gather.5
  222.0 11.0 reduce-scatter.4
  238.5 14.6 all-gather.3
  277.2 189.7 reduce-scatter.6
where the time goes:
time: 492 us; the launch traced here: 491 us
  waiting for transfers between devices  304 us (62%)
  blocking collectives  79.6 us (16%)
  matrix products  44.1 us (9%)
  other arithmetic  25.9 us (5%)
  local copies, waits for them, and re-layouts  17.5 us (4%)
  between operations  14 us (3%)
  starting transfers between devices  5.86 us (1%)
    all_gather x1, waiting for transfers between devices, in_one_piece(): lax.all_gather(both, axis, axis=dim, tiled=True)  176 us
    reduce_scatter x1, waiting for transfers between devices, body(): lax.psum_scatter(make_term(earlier_rows, d_gate, d_up).astype(jnp.bfloat1...  101 us
    psum x1, blocking collectives, body(): gain_sum = lax.psum(gain_local, ('rep', 'fs', 'tp'))  79.6 us
    unnamed x35, local copies, waits for them, and re-layouts  15.6 us
    all_gather x1, waiting for transfers between devices, body(): lax.all_gather(earlier_norm, 'tp', axis=0, tiled=True)  15 us
    concatenate x1, other arithmetic, make_term(): return jnp.concatenate([gate_part, up_part], axis=1)  13.8 us
    reduce_scatter x1, waiting for transfers between devices, body(): lax.psum_scatter((result + lax.dot_general(d_up, up_whole, CONTRACT_COLS,...  10.9 us
  transfers between devices with their start and end apart: 6, of which 5 were waited for; matrix products, arithmetic and copies ran while one was open for 11% of the time, Pallas kernels for 0%

commit v1 on v0

v1 whole, which is shorter than its diff:
```python
import functools
import math

import jax
import jax.numpy as jnp
from jax import lax
from jax.experimental import pallas as pl
from jax.experimental.pallas import tpu as pltpu
from jax.sharding import PartitionSpec as P

EPSILON = 1e-06
MESH = pl.DeviceIdType.MESH
HALF = 128
F32, BF16 = jnp.float32, jnp.bfloat16
SIZE = {"z": 2, "y": 4, "x": 4}
ORDERS = (("y", "z", "x"), ("x", "z", "y"), ("x", "y", "z"), ("y", "x", "z"))
ALL = slice(None)


def sigmoid(v):
    return 1.0 / (1.0 + jnp.exp(-v))


def landing_shapes(blocks, quarter):
    shapes = []
    for order in ORDERS:
        full = [a for a in "zyx"]
        for axis in reversed(order):
            full.remove(axis)
            lead = tuple(SIZE[a] for a in full)
            if axis == "z":
                shapes.append((blocks, 2, *lead, quarter, HALF))
            else:
                shapes.append((blocks, 2, *lead, quarter, HALF))
                shapes.append((blocks, 2, *lead, quarter, 2 * HALF))
    return shapes


def kernel(
    blocks, factor, later_hbm, earlier_hbm, cot_hbm, gain_ref, gw_hbm, uw_hbm, grun_hbm, urun_hbm, gain_run,
    hidden_hbm, grad_hbm, gtot_hbm, utot_hbm, gain_tot,
    w, g, xin, xl, xe, xt, cot, d, acc, lh, dn, inv_ref, run, gbuf, rep_in, *rest,
):
    landing = list(rest[:-10])
    ag_send, ag_recv, rs_send, rs_recv, load_sem, w_sem, tp_send, tp_recv, gs, out_sem = rest[-10:]
    gain_send, gain_recv = gs.at[0], gs.at[1]
    rows = xin.shape[1]
    width = xin.shape[2]
    quarter = g.shape[4] // 4
    rep, fs, tp = lax.axis_index("rep"), lax.axis_index("fs"), lax.axis_index("tp")
    own = {"x": fs % 4, "y": (fs // 4) % 4, "z": fs // 16}
    ring_z = 2 * rep + own["z"]

    def peer(axis, by):
        if axis == "z":
            z = (ring_z + by) % 4
            return {"rep": z // 2, "fs": (z % 2) * 16 + own["y"] * 4 + own["x"]}
        c = (own[axis] + by) % 4
        if axis == "y":
            return {"fs": own["z"] * 16 + c * 4 + own["x"]}
        return {"fs": own["z"] * 16 + own["y"] * 4 + c}

    def shifted(axis, by):
        return (1 - own["z"] if by else own["z"]) if axis == "z" else (own[axis] + by) % 4

    HALVES = (pl.ds(0, HALF), pl.ds(HALF, HALF), pl.ds(0, 2 * HALF))

    def region(j, q, sel, half):
        return (j, sel["z"], sel["y"], sel["x"], pl.ds(q * quarter, quarter), HALVES[half])

    def sel_of(full, axis, coordinate):
        s = {a: (ALL if a in full else own[a]) for a in "zyx"}
        s[axis] = coordinate
        return s

    ag_plan = []
    count = 0
    for q, order in enumerate(ORDERS):
        phases = []
        for p, axis in enumerate(order):
            full = order[:p]
            if axis == "z":
                group = []
                for k, by in enumerate((1, -1)):
                    group.append((count, (q, sel_of(full, "z", own["z"]), k), ("z", by), (q, sel_of(full, "z", 1 - own["z"]), k)))
                    count += 1
                phases.append(("z", [group]))
            else:
                first, second = [], []
                for k, by in enumerate((1, -1)):
                    first.append((count, (q, sel_of(full, axis, own[axis]), 2), (axis, by), (q, sel_of(full, axis, shifted(axis, -by)), 2)))
                    count += 1
                for k, by in enumerate((1, -1)):
                    second.append((count, (q, sel_of(full, axis, shifted(axis, -by)), k), (axis, by), (q, sel_of(full, axis, shifted(axis, 2)), k)))
                    count += 1
                phases.append((axis, [first, second]))
        ag_plan.append([group for _, groups in phases for group in groups])

    def ag_start(j, t):
        i, src, to, _ = t
        pltpu.make_async_remote_copy(
            src_ref=w.at[region(j, *src)], dst_ref=w.at[region(j, *src)], send_sem=ag_send.at[j, i], recv_sem=ag_recv.at[j, i],
            device_id=peer(*to), device_id_type=MESH,
        ).start()

    def ag_wait(j, t):
        i, src, to, dst = t
        pltpu.make_async_remote_copy(
            src_ref=w.at[region(j, *src)], dst_ref=w.at[region(j, *dst)], send_sem=ag_send.at[j, i], recv_sem=ag_recv.at[j, i],
            device_id=peer(*to), device_id_type=MESH,
        ).wait()

    def ag_stage(j, s):
        for plan in ag_plan:
            if s >= 1:
                for t in plan[s - 1]:
                    ag_wait(j, t)
            if s < len(plan):
                for t in plan[s]:
                    ag_start(j, t)

    rs_plan = []
    count, place = 0, 0
    for q, order in enumerate(ORDERS):
        groups = []
        full = ["z", "y", "x"]
        for axis in reversed(order):
            full.remove(axis)
            if axis == "z":
                group = []
                for k, by in enumerate((1, -1)):
                    group.append((count, (q, sel_of(full, "z", 1 - own["z"]), k), ("z", by), place, k, (q, sel_of(full, "z", own["z"]), k)))
                    count += 1
                groups.append(group)
                place += 1
            else:
                first, second = [], []
                for k, by in enumerate((1, -1)):
                    first.append((count, (q, sel_of(full, axis, shifted(axis, 2)), k), (axis, by), place, k, (q, sel_of(full, axis, shifted(axis, by)), k)))
                    count += 1
                for k, by in enumerate((1, -1)):
                    second.append((count, (q, sel_of(full, axis, shifted(axis, by)), 2), (axis, by), place + 1, k, (q, sel_of(full, axis, own[axis]), 2)))
                    count += 1
                groups += [first, second]
                place += 2
        rs_plan.append(groups)
    rep_index = count

    def rs_copy(j, t):
        i, src, to, at, slot, _ = t
        return pltpu.make_async_remote_copy(
            src_ref=g.at[region(j, *src)], dst_ref=landing[at].at[j, slot], send_sem=rs_send.at[j, i], recv_sem=rs_recv.at[j, i],
            device_id=peer(*to), device_id_type=MESH,
        )

    def rep_copy(j):
        return pltpu.make_async_remote_copy(
            src_ref=g.at[j, own["z"], own["y"], own["x"]], dst_ref=rep_in.at[j], send_sem=rs_send.at[j, rep_index],
            recv_sem=rs_recv.at[j, rep_index], device_id=peer("z", 2), device_id_type=MESH,
        )

    def rs_stage(j, s):
        for plan in rs_plan:
            if s >= 1:
                for t in plan[s - 1]:
                    rs_copy(j, t).wait()
                    _, _, _, at, slot, target = t
                    to = region(j, *target)
                    g[to] = (g[to].astype(F32) + landing[at][j, slot].astype(F32)).astype(BF16)
            if s < len(plan):
                for t in plan[s]:
                    rs_copy(j, t).start()
        if s == 5:
            rep_copy(j).start()

    def rs_finish(j):
        rep_copy(j).wait()
        total = g[j, own["z"], own["y"], own["x"]].astype(F32) + rep_in[j].astype(F32)
        columns = pl.ds(pl.multiple_of(j * HALF, HALF), HALF)
        run[0, :, columns] = run[0, :, columns] + factor * total[:, :HALF]
        run[1, :, columns] = run[1, :, columns] + factor * total[:, HALF:]

    def tp_copy(i, ref):
        return pltpu.make_async_remote_copy(
            src_ref=ref, dst_ref=ref, send_sem=tp_send.at[i], recv_sem=tp_recv.at[i], device_id={"tp": 1 - tp}, device_id_type=MESH
        )

    def tp_received(i, ref):
        return pltpu.make_async_remote_copy(
            src_ref=ref, dst_ref=ref, send_sem=tp_send.at[i], recv_sem=tp_recv.at[i], device_id={"tp": 1 - tp}, device_id_type=MESH
        )

    def dn_copy():
        return pltpu.make_async_remote_copy(
            src_ref=dn.at[1], dst_ref=dn.at[2], send_sem=tp_send.at[3], recv_sem=tp_recv.at[3], device_id={"tp": 1 - tp}, device_id_type=MESH
        )

    loads = [
        pltpu.make_async_copy(later_hbm, xin.at[0], load_sem.at[0]),
        pltpu.make_async_copy(earlier_hbm, xin.at[1], load_sem.at[1]),
        pltpu.make_async_copy(cot_hbm, cot, load_sem.at[2]),
        pltpu.make_async_copy(grun_hbm, run.at[0], load_sem.at[3]),
        pltpu.make_async_copy(urun_hbm, run.at[1], load_sem.at[4]),
    ]

    def shard_loads(j):
        columns = pl.ds(pl.multiple_of(j * HALF, HALF), HALF)
        mine = (j, own["z"], own["y"], own["x"], ALL)
        return [
            pltpu.make_async_copy(gw_hbm.at[:, columns], w.at[(*mine, pl.ds(0, HALF))], w_sem.at[0, j]),
            pltpu.make_async_copy(uw_hbm.at[:, columns], w.at[(*mine, pl.ds(HALF, HALF))], w_sem.at[1, j]),
        ]

    @pl.loop(0, blocks)
    def _(j):
        for c in shard_loads(j):
            c.start()

    for c in loads:
        c.start()

    barrier = pltpu.get_barrier_semaphore()
    greeted = [peer(a, by) for a in "xyz" for by in (1, 2, 3)] + [{"tp": 1 - tp}]
    for device in greeted:
        pl.semaphore_signal(barrier, inc=1, device_id=device, device_id_type=MESH)
    pl.semaphore_wait(barrier, len(greeted))

    @pl.loop(0, blocks)
    def _(j):
        for c in shard_loads(j):
            c.wait()

    step_rows = 32 if rows % 32 == 0 else rows

    def normalize():
        for c in loads:
            c.wait()

        @pl.loop(0, rows // step_rows)
        def _(i):
            at = pl.ds(pl.multiple_of(i * step_rows, step_rows), step_rows)
            for m, out in ((0, xl), (1, xe)):
                values = xin[m, at, :].astype(F32)
                inv = lax.rsqrt(jnp.mean(values * values, axis=1, keepdims=True) + EPSILON)
                out[tp, at, :] = (values * inv * gain_ref[...]).astype(BF16)
                if m == 1:
                    inv_ref[at, :] = inv

        tp_copy(0, xl.at[tp]).start()
        tp_copy(1, xe.at[tp]).start()
        slab = min(256, width)

        @pl.loop(0, width // slab)
        def _(i):
            at = pl.ds(pl.multiple_of(i * slab, slab), slab)
            xt[tp, at, :] = xe[tp, :, at].T

        tp_copy(2, xt.at[tp]).start()
        acc[...] = jnp.zeros_like(acc)

    def exchanged():
        for i, ref in ((0, xl), (1, xe), (2, xt)):
            tp_copy(i, ref.at[tp]).wait_send()
            tp_received(i, ref.at[1 - tp]).wait_recv()

    def block_weight(j):
        return w[j].reshape(width, 2 * HALF)

    def backward(j):
        columns = pl.ds(pl.multiple_of(j * HALF, HALF), HALF)

        @pl.loop(0, 2)
        def _(m):
            both = jnp.dot(xe[m], block_weight(j), preferred_element_type=F32)
            gate, up = both[:, :HALF], both[:, HALF:]
            s = sigmoid(gate)
            c = cot[pl.ds(pl.multiple_of(m * rows, rows), rows), columns].astype(F32)
            d[m, :, 0:HALF] = (c * up * s * (1.0 + gate * (1.0 - s))).astype(BF16)
            d[m, :, HALF:] = (c * gate * s).astype(BF16)

        @pl.loop(0, 4)
        def _(k):
            z, y = k // 2, 2 * (k % 2)
            at = pl.ds(pl.multiple_of(k * (width // 4), width // 4), width // 4)
            part = jnp.dot(xt[0, at, :], d[0], preferred_element_type=F32)
            part = part + jnp.dot(xt[1, at, :], d[1], preferred_element_type=F32)
            g[j, z, pl.ds(y, 2)] = part.astype(BF16).reshape(2, 4, 4 * quarter, 2 * HALF)

    def later(j):
        @pl.loop(0, 2)
        def _(m):
            both = jnp.dot(xl[m], block_weight(j), preferred_element_type=F32)
            gate, up = both[:, :HALF], both[:, HALF:]
            lh[j, pl.ds(pl.multiple_of(m * rows, rows), rows), :] = (gate * sigmoid(gate) * up).astype(BF16)

        hidden_copy(j).start()

    def hidden_copy(j):
        columns = pl.ds(pl.multiple_of(j * HALF, HALF), HALF)
        return pltpu.make_async_copy(lh.at[j], hidden_hbm.at[:, columns], out_sem.at[j])

    def input_gradient(j):
        @pl.loop(0, 4)
        def _(k):
            z, y = k // 2, 2 * (k % 2)
            at = pl.ds(pl.multiple_of(k * (width // 4), width // 4), width // 4)
            part = w[j, z, pl.ds(y, 2)].reshape(width // 4, 2 * HALF)
            for m in range(2):
                acc[m, :, at] = acc[m, :, at] + lax.dot_general(
                    d[m], part, (((1,), (1,)), ((), ())), preferred_element_type=F32
                )

    def send_input_gradient():
        @pl.loop(0, rows // step_rows)
        def _(i):
            at = pl.ds(pl.multiple_of(i * step_rows, step_rows), step_rows)
            dn[0, at, :] = acc[tp, at, :].astype(BF16)
            dn[1, at, :] = acc[1 - tp, at, :].astype(BF16)

        dn_copy().start()

    def finish_input_gradient():
        dn_copy().wait()
        gain = gain_ref[...]
        own_slot = gbuf.at[0, own["x"]]
        own_slot[...] = jnp.zeros_like(own_slot)

        @pl.loop(0, rows // step_rows)
        def _(i):
            at = pl.ds(pl.multiple_of(i * step_rows, step_rows), step_rows)
            d_norm = dn[0, at, :].astype(F32) + dn[2, at, :].astype(F32)
            values = xin[1, at, :].astype(F32)
            inv = inv_ref[at, :]
            scaled = d_norm * gain
            inner = jnp.mean(scaled * values, axis=1, keepdims=True)
            dn[1, at, :] = (inv * scaled - values * (inv * inv * inv) * inner).astype(BF16)
            own_slot[...] = own_slot[...] + jnp.sum(d_norm * values * inv, axis=0, keepdims=True)

        grad_copy().start()

    def grad_copy():
        return pltpu.make_async_copy(dn.at[1], grad_hbm, out_sem.at[blocks])

    def gain_copies(r):
        axis = ("x", "y", "z")[r]
        at = (own["x"], own["y"], ring_z)[r]
        return [
            pltpu.make_async_remote_copy(
                src_ref=gbuf.at[r, at], dst_ref=gbuf.at[r, at], send_sem=gain_send.at[r, k], recv_sem=gain_recv.at[r, k],
                device_id=peer(axis, k), device_id_type=MESH,
            )
            for k in (1, 2, 3)
        ]

    def gain_received(r):
        axis = ("x", "y", "z")[r]
        at = (own["x"], own["y"], ring_z)[r]
        return [
            pltpu.make_async_remote_copy(
                src_ref=gbuf.at[r, at], dst_ref=gbuf.at[r, (at - k) % 4], send_sem=gain_send.at[r, k], recv_sem=gain_recv.at[r, k],
                device_id=peer(axis, k), device_id_type=MESH,
            )
            for k in (1, 2, 3)
        ]

    def gain_sum(r):
        for c in gain_received(r):
            c.wait()
        return (gbuf[r, 0] + gbuf[r, 1]) + (gbuf[r, 2] + gbuf[r, 3])

    def gain_tp():
        return pltpu.make_async_remote_copy(
            src_ref=gbuf.at[3, 0], dst_ref=gbuf.at[3, 1], send_sem=gain_send.at[3, 1], recv_sem=gain_recv.at[3, 1],
            device_id={"tp": 1 - tp}, device_id_type=MESH,
        )

    def gain_step(r):
        if r == 0:
            finish_input_gradient()
            for c in gain_copies(0):
                c.start()
        elif r < 3:
            gbuf[r, (own["x"], own["y"], ring_z)[r]] = gain_sum(r - 1)
            for c in gain_copies(r):
                c.start()
        elif r == 3:
            gbuf[3, 0] = gain_sum(2)
            gain_tp().start()
        else:
            gain_tp().wait()
            gain_tot[...] = gain_run[...] + factor * (gbuf[3, 0] + gbuf[3, 1])

    last = 5 + blocks - 1

    @pl.loop(0, last + 8)
    def _(t):
        def at_stage(offset, run_stage):
            j = t - offset

            @pl.when((j >= 0) & (j < blocks))
            def _():
                run_stage(j)

        for s in (1, 2, 3, 4, 0):
            at_stage(s, functools.partial(ag_stage, s=s))
        for s in (1, 2, 3, 4, 5):
            at_stage(5 + s, functools.partial(rs_stage, s=s))
        at_stage(11, rs_finish)

        @pl.when(t == 0)
        def _():
            normalize()

        @pl.when(t == 4)
        def _():
            exchanged()

        def compute(j):
            ag_stage(j, 5)
            backward(j)
            rs_stage(j, 0)
            later(j)
            input_gradient(j)

        at_stage(5, compute)

        @pl.when(t == last)
        def _():
            send_input_gradient()

        for r in range(5):
            @pl.when(t == last + 1 + r)
            def _():
                gain_step(r)

    outs = [pltpu.make_async_copy(run.at[0], gtot_hbm, load_sem.at[0]), pltpu.make_async_copy(run.at[1], utot_hbm, load_sem.at[1])]
    for c in outs:
        c.start()

    @pl.loop(0, blocks)
    def _(j):
        hidden_copy(j).wait()

    grad_copy().wait()
    for c in outs:
        c.wait()


def body(later_input, earlier_input, hidden_cot, norm_gain, gate_weight, up_weight, gate_running, up_running, gain_running):
    rows, width = later_input.shape
    shard, hidden = gate_weight.shape
    blocks = hidden // HALF
    quarter = shard // 4
    tokens = rows * lax.axis_size("rep") * lax.axis_size("fs") * lax.axis_size("tp")
    factor = 1.0 / math.sqrt(tokens)
    whole = (blocks, 2, 4, 4, shard, 2 * HALF)
    hbm = pl.BlockSpec(memory_space=pl.ANY)
    vmem = pl.BlockSpec(memory_space=pltpu.VMEM)
    dma = pltpu.SemaphoreType.DMA
    out = pl.pallas_call(
        functools.partial(kernel, blocks, factor),
        out_shape=(
            jax.ShapeDtypeStruct((2 * rows, hidden), BF16),
            jax.ShapeDtypeStruct((rows, width), BF16),
            jax.ShapeDtypeStruct((shard, hidden), F32),
            jax.ShapeDtypeStruct((shard, hidden), F32),
            jax.ShapeDtypeStruct((1, width), F32),
        ),
        in_specs=[hbm, hbm, hbm, vmem, hbm, hbm, hbm, hbm, vmem],
        out_specs=(hbm, hbm, hbm, hbm, vmem),
        scratch_shapes=[
            pltpu.VMEM(whole, BF16),
            pltpu.VMEM(whole, BF16),
            pltpu.VMEM((2, rows, width), BF16),
            pltpu.VMEM((2, rows, width), BF16),
            pltpu.VMEM((2, rows, width), BF16),
            pltpu.VMEM((2, width, rows), BF16),
            pltpu.VMEM((2 * rows, hidden), BF16),
            pltpu.VMEM((2, rows, 2 * HALF), BF16),
            pltpu.VMEM((2, rows, width), F32),
            pltpu.VMEM((blocks, 2 * rows, HALF), BF16),
            pltpu.VMEM((3, rows, width), BF16),
            pltpu.VMEM((rows, 1), F32),
            pltpu.VMEM((2, shard, hidden), F32),
            pltpu.VMEM((4, 4, 1, width), F32),
            pltpu.VMEM((blocks, shard, 2 * HALF), BF16),
            *[pltpu.VMEM(s, BF16) for s in landing_shapes(blocks, quarter)],
            dma((blocks, 40)),
            dma((blocks, 40)),
            dma((blocks, 41)),
            dma((blocks, 41)),
            dma((5,)),
            dma((2, blocks)),
            dma((4,)),
            dma((4,)),
            dma((2, 4, 4)),
            dma((blocks + 1,)),
        ],
        compiler_params=pltpu.CompilerParams(collective_id=0, has_side_effects=True, vmem_limit_bytes=67043328),
        cost_estimate=pl.CostEstimate(flops=16 * rows * width * hidden * 2, bytes_accessed=16 << 20, transcendentals=0),
        name="half_step",
    )(
        later_input, earlier_input, hidden_cot, norm_gain.reshape(1, width), gate_weight, up_weight, gate_running, up_running,
        gain_running.reshape(1, width),
    )
    hidden_out, grad, gate_total, up_total, gain_total = out
    return hidden_out, grad, gate_total, up_total, gain_total.reshape(width)


def solution(mesh):
    in_specs = (
        P(("rep", "fs", "tp"), None),
        P(("rep", "fs", "tp"), None),
        P(("rep", "fs"), "tp"),
        P(),
        P("fs", "tp"),
        P("fs", "tp"),
        P("fs", "tp"),
        P("fs", "tp"),
        P(),
    )
    out_specs = (
        P(("rep", "fs"), "tp"),
        P(("rep", "fs", "tp"), None),
        P("fs", "tp"),
        P("fs", "tp"),
        P(),
    )
    return jax.shard_map(body, mesh=mesh, in_specs=in_specs, out_specs=out_specs, check_vma=False)
```

time: 492 us -> 161 us (0.33)
  waiting for transfers between devices: 304 us -> 0 us
  Pallas kernels: 0 us -> 154 us
  blocking collectives: 79.6 us -> 0 us
  matrix products: 44.1 us -> 0 us
  other arithmetic: 25.9 us -> 0 us
  between operations: 14 us -> 0.66 us
  local copies, waits for them, and re-layouts: 17.5 us -> 5.9 us
  starting transfers between devices: 5.86 us -> 0 us
    all_gather x3 -> x0, waiting for transfers between devices: 191 us -> none  [the longest x1 176 us: in_one_piece(): lax.all_gather(both, axis, axis=dim, tiled=True)]
    pallas_call x0 -> x1, Pallas kernels: none -> 154 us  [body(): pl.pallas_call(functools.partial(kernel, blocks, factor), out_shape=(jax....]
    reduce_scatter x2 -> x0, waiting for transfers between devices: 112 us -> none  [the longest x1 101 us: body(): lax.psum_scatter(make_term(earlier_rows, d_gate, d_up).astype(jnp.bfloat1...]
    psum x1 -> x0, blocking collectives: 79.6 us -> none  [body(): gain_sum = lax.psum(gain_local, ('rep', 'fs', 'tp'))]
    dot_general x8 -> x0, matrix products: 44.1 us -> none  [the longest x1 8.52 us: body(): jnp.dot(later_rows, gate_whole, preferred_element_type=jnp.float32)]
    concatenate x2 -> x0, other arithmetic: 14.6 us -> none  [the longest x1 13.8 us: make_term(): return jnp.concatenate([gate_part, up_part], axis=1)]
    unnamed x35 -> x13, local copies, waits for them, and re-layouts: 15.6 us -> 5.9 us
    convert_element_type x2 -> x0, other arithmetic: 5.84 us -> none  [the longest x1 3.33 us: body(): (earlier_inv * scaled - earlier_vals * earlier_inv ** 3 * inner).astype(j...]
  transfers between devices with their start and end apart: 6 -> 0, of which waited for: 5 -> 0; matrix products, arithmetic and copies ran while one was open for 11% -> 0% of each run, Pallas kernels for 0% -> 0%
where the time goes in v1:
time: 161 us
  Pallas kernels  154 us (96%)
  local copies, waits for them, and re-layouts  5.9 us (4%)
    pallas_call x1, Pallas kernels, body(): pl.pallas_call(functools.partial(kernel, blocks, factor), out_shape=(jax....  154 us
    unnamed x13, local copies, waits for them, and re-layouts  5.9 us

profile of v1, /device:TPU:0, one launch (start us, length us, event | category | flops | bytes accessed | tf_op | source)
XLA Modules:
  0.0 160.6 jit_solution(13597032927552643515)
XLA Ops:
  0.6 154.1 %half_step.1 = (bf16[512,1408]{1,0:T(8,128)(2,1)}, bf16[256,2048]{1,0:T(8,128)(2,1)}, f32[64,1408]{1,0:T(8,128)}, f32[64,1408]{1,0:T(8,128)}, f32[1,2048]{1,0:T(1,128)}) custom-call(bf16[256,2048]{1,0:T(8,128)(2,1)} %later_hbm.1, bf16[256,2048]{1,0:T(8,128)(2,1)} %earlier_hbm.1, bf16[512,1408]{1,0:T(8,128)(2,1)} %cot_hbm.1, f32[1,2048]{1,0:T(1,128)} %bitcast.4, ...), custom_call_target="tpu_custom_call" | custom-call | flops 23622320128 | bytes 16777216 | tf_op jit(solution)/shard_map/half_step/pallas_call | solution.py:460
  154.7 0.0 copy-start
  154.7 2.7 %copy.19 = bf16[512,1408]{1,0:T(8,128)(2,1)} copy(bf16[512,1408]{1,0:T(8,128)(2,1)} %get-tuple-element.20) | data formatting | bytes 2883584
  157.4 0.0 copy-done
  157.4 0.0 copy-start.2
  157.4 0.0 copy-start.1
  157.4 0.0 copy-start.3
  157.4 1.0 copy.20
  158.3 0.2 copy-done.2
  158.5 0.7 copy.21
  159.3 0.0 copy-done.1
  159.3 0.7 copy.22
  160.0 0.0 copy-done.3
  160.0 0.6 copy.23
Async XLA Ops:
  154.7 2.7 %copy-start = (bf16[256,2048]{1,0:T(8,128)(2,1)S(1)}, bf16[256,2048]{1,0:T(8,128)(2,1)}, u32[]{:S(2)}) copy-start(bf16[256,2048]{1,0:T(8,128)(2,1)} %get-tuple-element.21) | copy-start | bytes 3145732
  157.4 1.2 copy-start.2
  157.4 1.9 %copy-start.1 = (f32[64,1408]{1,0:T(8,128)S(1)}, f32[64,1408]{1,0:T(8,128)}, u32[]{:S(2)}) copy-start(f32[64,1408]{1,0:T(8,128)} %get-tuple-element.23) | copy-start | bytes 1081348
  157.4 2.6 %copy-start.3 = (f32[1,2048]{1,0:T(1,128)S(1)}, f32[1,2048]{1,0:T(1,128)}, u32[]{:S(2)}) copy-start(f32[1,2048]{1,0:T(1,128)} %get-tuple-element.14) | copy-start | bytes 24580

commit v2 on v1

--- a/solution.py
+++ b/solution.py
@@ -15,6 +15,8 @@
 SIZE = {"z": 2, "y": 4, "x": 4}
 ORDERS = (("y", "z", "x"), ("x", "z", "y"), ("x", "y", "z"), ("y", "x", "z"))
 ALL = slice(None)
+AG_SHARDS = (2, 1, 6, 10, 12)
+RS_SHARDS = (12, 10, 6, 1, 2)
 
 
 def sigmoid(v):
@@ -96,28 +98,31 @@
                 phases.append((axis, [first, second]))
         ag_plan.append([group for _, groups in phases for group in groups])
 
-    def ag_start(j, t):
-        i, src, to, _ = t
+    def shards(n):
+        if n <= 4:
+            return w.at[0, 0, 0, pl.ds(0, n)]
+        if n % 4 == 0:
+            return w.at[0, 0, pl.ds(0, n // 4)]
+        return w.at[pl.ds(0, n // 2), :, 0, 0]
+
+    def await_stage(n, send, recv):
+        pltpu.make_async_copy(shards(n), shards(n), send).wait()
+        pltpu.make_async_copy(shards(n), shards(n), recv).wait()
+
+    def ag_start(j, s, t):
+        _, src, to, _ = t
         pltpu.make_async_remote_copy(
-            src_ref=w.at[region(j, *src)], dst_ref=w.at[region(j, *src)], send_sem=ag_send.at[j, i], recv_sem=ag_recv.at[j, i],
+            src_ref=w.at[region(j, *src)], dst_ref=w.at[region(j, *src)], send_sem=ag_send.at[s], recv_sem=ag_recv.at[j % 2, s],
             device_id=peer(*to), device_id_type=MESH,
         ).start()
 
-    def ag_wait(j, t):
-        i, src, to, dst = t
-        pltpu.make_async_remote_copy(
-            src_ref=w.at[region(j, *src)], dst_ref=w.at[region(j, *dst)], send_sem=ag_send.at[j, i], recv_sem=ag_recv.at[j, i],
-            device_id=peer(*to), device_id_type=MESH,
-        ).wait()
-
     def ag_stage(j, s):
-        for plan in ag_plan:
-            if s >= 1:
-                for t in plan[s - 1]:
-                    ag_wait(j, t)
-            if s < len(plan):
+        if s >= 1:
+            await_stage(AG_SHARDS[s - 1], ag_send.at[s - 1], ag_recv.at[j % 2, s - 1])
+        if s < 5:
+            for plan in ag_plan:
                 for t in plan[s]:
-                    ag_start(j, t)
+                    ag_start(j, s, t)
 
     rs_plan = []
     count, place = 0, 0
@@ -144,32 +149,31 @@
                 groups += [first, second]
                 place += 2
         rs_plan.append(groups)
-    rep_index = count
-
-    def rs_copy(j, t):
-        i, src, to, at, slot, _ = t
-        return pltpu.make_async_remote_copy(
-            src_ref=g.at[region(j, *src)], dst_ref=landing[at].at[j, slot], send_sem=rs_send.at[j, i], recv_sem=rs_recv.at[j, i],
+
+    def rs_start(j, s, t):
+        _, src, to, at, slot, _ = t
+        pltpu.make_async_remote_copy(
+            src_ref=g.at[region(j, *src)], dst_ref=landing[at].at[j, slot], send_sem=rs_send.at[s], recv_sem=rs_recv.at[j % 2, s],
             device_id=peer(*to), device_id_type=MESH,
-        )
+        ).start()
 
     def rep_copy(j):
         return pltpu.make_async_remote_copy(
-            src_ref=g.at[j, own["z"], own["y"], own["x"]], dst_ref=rep_in.at[j], send_sem=rs_send.at[j, rep_index],
-            recv_sem=rs_recv.at[j, rep_index], device_id=peer("z", 2), device_id_type=MESH,
+            src_ref=g.at[j, own["z"], own["y"], own["x"]], dst_ref=rep_in.at[j], send_sem=rs_send.at[5],
+            recv_sem=rs_recv.at[j % 2, 5], device_id=peer("z", 2), device_id_type=MESH,
         )
 
     def rs_stage(j, s):
+        if s >= 1:
+            await_stage(RS_SHARDS[s - 1], rs_send.at[s - 1], rs_recv.at[j % 2, s - 1])
         for plan in rs_plan:
             if s >= 1:
-                for t in plan[s - 1]:
-                    rs_copy(j, t).wait()
-                    _, _, _, at, slot, target = t
+                for _, _, _, at, slot, target in plan[s - 1]:
                     to = region(j, *target)
                     g[to] = (g[to].astype(F32) + landing[at][j, slot].astype(F32)).astype(BF16)
-            if s < len(plan):
+            if s < 5:
                 for t in plan[s]:
-                    rs_copy(j, t).start()
+                    rs_start(j, s, t)
         if s == 5:
             rep_copy(j).start()
 
@@ -232,31 +236,38 @@
 
     step_rows = 32 if rows % 32 == 0 else rows
 
-    def normalize():
-        for c in loads:
-            c.wait()
-
+    def normalize(m, out):
         @pl.loop(0, rows // step_rows)
         def _(i):
             at = pl.ds(pl.multiple_of(i * step_rows, step_rows), step_rows)
-            for m, out in ((0, xl), (1, xe)):
-                values = xin[m, at, :].astype(F32)
-                inv = lax.rsqrt(jnp.mean(values * values, axis=1, keepdims=True) + EPSILON)
-                out[tp, at, :] = (values * inv * gain_ref[...]).astype(BF16)
-                if m == 1:
-                    inv_ref[at, :] = inv
-
-        tp_copy(0, xl.at[tp]).start()
-        tp_copy(1, xe.at[tp]).start()
-        slab = min(256, width)
-
-        @pl.loop(0, width // slab)
-        def _(i):
-            at = pl.ds(pl.multiple_of(i * slab, slab), slab)
-            xt[tp, at, :] = xe[tp, :, at].T
-
-        tp_copy(2, xt.at[tp]).start()
-        acc[...] = jnp.zeros_like(acc)
+            values = xin[m, at, :].astype(F32)
+            inv = lax.rsqrt(jnp.mean(values * values, axis=1, keepdims=True) + EPSILON)
+            out[tp, at, :] = (values * inv * gain_ref[...]).astype(BF16)
+            if m == 1:
+                inv_ref[at, :] = inv
+
+    def prepare(t):
+        if t == 0:
+            for c in loads:
+                c.wait()
+            normalize(1, xe)
+            tp_copy(1, xe.at[tp]).start()
+        elif t == 1:
+            slab = min(256, width)
+
+            @pl.loop(0, width // slab)
+            def _(i):
+                at = pl.ds(pl.multiple_of(i * slab, slab), slab)
+                xt[tp, at, :] = xe[tp, :, at].T
+
+            tp_copy(2, xt.at[tp]).start()
+        elif t == 2:
+            normalize(0, xl)
+            tp_copy(0, xl.at[tp]).start()
+        elif t == 3:
+            acc[...] = jnp.zeros_like(acc)
+        else:
+            exchanged()
 
     def exchanged():
         for i, ref in ((0, xl), (1, xe), (2, xt)):
@@ -401,22 +412,18 @@
             def _():
                 run_stage(j)
 
-        for s in (1, 2, 3, 4, 0):
+        for s in (5, 4, 3, 2, 1, 0):
             at_stage(s, functools.partial(ag_stage, s=s))
-        for s in (1, 2, 3, 4, 5):
+        at_stage(11, rs_finish)
+        for s in (5, 4, 3, 2, 1):
             at_stage(5 + s, functools.partial(rs_stage, s=s))
-        at_stage(11, rs_finish)
-
-        @pl.when(t == 0)
-        def _():
-            normalize()
-
-        @pl.when(t == 4)
-        def _():
-            exchanged()
+
+        for k in range(5):
+            @pl.when(t == k)
+            def _():
+                prepare(k)
 
         def compute(j):
-            ag_stage(j, 5)
             backward(j)
             rs_stage(j, 0)
             later(j)
@@ -485,10 +492,10 @@
             pltpu.VMEM((4, 4, 1, width), F32),
             pltpu.VMEM((blocks, shard, 2 * HALF), BF16),
             *[pltpu.VMEM(s, BF16) for s in landing_shapes(blocks, quarter)],
-            dma((blocks, 40)),
-            dma((blocks, 40)),
-            dma((blocks, 41)),
-            dma((blocks, 41)),
+            dma((5,)),
+            dma((2, 5)),
+            dma((6,)),
+            dma((2, 6)),
             dma((5,)),
             dma((2, blocks)),
             dma((4,)),

time: 161 us -> 142 us (0.88)
  Pallas kernels: 154 us -> 136 us
    pallas_call x1, Pallas kernels: 154 us -> 136 us  [body(): pl.pallas_call(functools.partial(kernel, blocks, factor), out_shape=(jax....]
where the time goes in v2:
time: 142 us
  Pallas kernels  136 us (96%)
  local copies, waits for them, and re-layouts  5.9 us (4%)
    pallas_call x1, Pallas kernels, body(): pl.pallas_call(functools.partial(kernel, blocks, factor), out_shape=(jax....  136 us
    unnamed x13, local copies, waits for them, and re-layouts  5.9 us

profile of v2, /device:TPU:0, one launch (start us, length us, event | category | flops | bytes accessed | tf_op | source)
XLA Modules:
  0.0 142.1 jit_solution(2184669864885376764)
XLA Ops:
  0.6 135.6 %half_step.1 = (bf16[512,1408]{1,0:T(8,128)(2,1)}, bf16[256,2048]{1,0:T(8,128)(2,1)}, f32[64,1408]{1,0:T(8,128)}, f32[64,1408]{1,0:T(8,128)}, f32[1,2048]{1,0:T(1,128)}) custom-call(bf16[256,2048]{1,0:T(8,128)(2,1)} %later_hbm.1, bf16[256,2048]{1,0:T(8,128)(2,1)} %earlier_hbm.1, bf16[512,1408]{1,0:T(8,128)(2,1)} %cot_hbm.1, f32[1,2048]{1,0:T(1,128)} %bitcast.4, ...), custom_call_target="tpu_custom_call" | custom-call | flops 23622320128 | bytes 16777216 | tf_op jit(solution)/shard_map/half_step/pallas_call | solution.py:467
  136.2 0.0 copy-start
  136.2 2.7 %copy.19 = bf16[512,1408]{1,0:T(8,128)(2,1)} copy(bf16[512,1408]{1,0:T(8,128)(2,1)} %get-tuple-element.20) | data formatting | bytes 2883584
  138.9 0.0 copy-done
  138.9 0.0 copy-start.2
  138.9 0.0 copy-start.1
  138.9 0.0 copy-start.3
  138.9 1.0 copy.20
  139.9 0.2 copy-done.2
  140.1 0.7 copy.21
  140.8 0.0 copy-done.1
  140.8 0.7 copy.22
  141.5 0.0 copy-done.3
  141.5 0.6 copy.23
Async XLA Ops:
  136.2 2.7 %copy-start = (bf16[256,2048]{1,0:T(8,128)(2,1)S(1)}, bf16[256,2048]{1,0:T(8,128)(2,1)}, u32[]{:S(2)}) copy-start(bf16[256,2048]{1,0:T(8,128)(2,1)} %get-tuple-element.21) | copy-start | bytes 3145732
  138.9 1.2 copy-start.2
  138.9 1.9 %copy-start.1 = (f32[64,1408]{1,0:T(8,128)S(1)}, f32[64,1408]{1,0:T(8,128)}, u32[]{:S(2)}) copy-start(f32[64,1408]{1,0:T(8,128)} %get-tuple-element.23) | copy-start | bytes 1081348
  138.9 2.6 %copy-start.3 = (f32[1,2048]{1,0:T(1,128)S(1)}, f32[1,2048]{1,0:T(1,128)}, u32[]{:S(2)}) copy-start(f32[1,2048]{1,0:T(1,128)} %get-tuple-element.14) | copy-start | bytes 24580

commit v3 on v2

--- a/solution.py
+++ b/solution.py
@@ -15,8 +15,8 @@
 SIZE = {"z": 2, "y": 4, "x": 4}
 ORDERS = (("y", "z", "x"), ("x", "z", "y"), ("x", "y", "z"), ("y", "x", "z"))
 ALL = slice(None)
-AG_SHARDS = (2, 1, 6, 10, 12)
-RS_SHARDS = (12, 10, 6, 1, 2)
+AG_SHARDS = ((1, 1), (0.5, 0.5), (2, 4), (8, 2), (4, 8))
+RS_SHARDS = ((4, 8), (8, 2), (2, 4), (0.5, 0.5), (1, 1))
 
 
 def sigmoid(v):
@@ -43,8 +43,8 @@
     hidden_hbm, grad_hbm, gtot_hbm, utot_hbm, gain_tot,
     w, g, xin, xl, xe, xt, cot, d, acc, lh, dn, inv_ref, run, gbuf, rep_in, *rest,
 ):
-    landing = list(rest[:-10])
-    ag_send, ag_recv, rs_send, rs_recv, load_sem, w_sem, tp_send, tp_recv, gs, out_sem = rest[-10:]
+    last_in, landing = rest[0], list(rest[1:-11])
+    ag_send, ag_recv, rs_send, rs_recv, once, load_sem, w_sem, tp_send, tp_recv, gs, out_sem = rest[-11:]
     gain_send, gain_recv = gs.at[0], gs.at[1]
     rows = xin.shape[1]
     width = xin.shape[2]
@@ -100,29 +100,46 @@
 
     def shards(n):
         if n <= 4:
+            if n == 0.5:
+                return w.at[0, 0, 0, 0, pl.ds(0, 2 * quarter)]
             return w.at[0, 0, 0, pl.ds(0, n)]
         if n % 4 == 0:
             return w.at[0, 0, pl.ds(0, n // 4)]
-        return w.at[pl.ds(0, n // 2), :, 0, 0]
+        return w.at[:, 0, 0, 0]
 
     def await_stage(n, send, recv):
         pltpu.make_async_copy(shards(n), shards(n), send).wait()
         pltpu.make_async_copy(shards(n), shards(n), recv).wait()
 
-    def ag_start(j, s, t):
-        _, src, to, _ = t
+    def ag_send_to(j, src, to, send, recv):
         pltpu.make_async_remote_copy(
-            src_ref=w.at[region(j, *src)], dst_ref=w.at[region(j, *src)], send_sem=ag_send.at[s], recv_sem=ag_recv.at[j % 2, s],
-            device_id=peer(*to), device_id_type=MESH,
+            src_ref=w.at[region(j, *src)], dst_ref=w.at[region(j, *src)], send_sem=send, recv_sem=recv, device_id=peer(*to), device_id_type=MESH
         ).start()
 
-    def ag_stage(j, s):
-        if s >= 1:
-            await_stage(AG_SHARDS[s - 1], ag_send.at[s - 1], ag_recv.at[j % 2, s - 1])
-        if s < 5:
-            for plan in ag_plan:
-                for t in plan[s]:
-                    ag_start(j, s, t)
+    def ag_stage(j, s, wait=True):
+        for pair in (1, 0):
+            if s >= 1 and wait:
+                await_stage(AG_SHARDS[s - 1][pair], ag_send.at[pair, s - 1], ag_recv.at[j % 2, pair, s - 1])
+            if s < 5:
+                for plan in ag_plan[2 * pair : 2 * pair + 2]:
+                    for _, src, to, _ in plan[s]:
+                        ag_send_to(j, src, to, ag_send.at[pair, s], ag_recv.at[j % 2, pair, s])
+
+    def ag_first():
+        for q, order in enumerate(ORDERS):
+            src = (q, sel_of((), order[0], own[order[0]]), 2)
+            for by in (2, 1, -1):
+                ag_send_to(0, src, (order[0], by), once.at[0], once.at[1])
+
+    def ag_second(j):
+        @pl.when(j == 0)
+        def _():
+            await_stage(3, once.at[0], once.at[1])
+            ag_stage(j, 2, wait=False)
+
+        @pl.when(j > 0)
+        def _():
+            ag_stage(j, 2)
 
     rs_plan = []
     count, place = 0, 0
@@ -150,35 +167,74 @@
                 place += 2
         rs_plan.append(groups)
 
-    def rs_start(j, s, t):
+    def rs_start(j, s, pair, t):
         _, src, to, at, slot, _ = t
         pltpu.make_async_remote_copy(
-            src_ref=g.at[region(j, *src)], dst_ref=landing[at].at[j, slot], send_sem=rs_send.at[s], recv_sem=rs_recv.at[j % 2, s],
+            src_ref=g.at[region(j, *src)], dst_ref=landing[at].at[j, slot], send_sem=rs_send.at[pair, s], recv_sem=rs_recv.at[j % 2, pair, s],
             device_id=peer(*to), device_id_type=MESH,
         ).start()
 
-    def rep_copy(j):
+    def rep_copy(j, send, recv):
         return pltpu.make_async_remote_copy(
-            src_ref=g.at[j, own["z"], own["y"], own["x"]], dst_ref=rep_in.at[j], send_sem=rs_send.at[5],
-            recv_sem=rs_recv.at[j % 2, 5], device_id=peer("z", 2), device_id_type=MESH,
+            src_ref=g.at[j, own["z"], own["y"], own["x"]], dst_ref=rep_in.at[j], send_sem=send, recv_sem=recv,
+            device_id=peer("z", 2), device_id_type=MESH,
         )
 
+    def rep_sems(j):
+        return rs_send.at[0, 5], rs_recv.at[j % 2, 0, 5]
+
+    def rs_collect(j, s, pair):
+        await_stage(RS_SHARDS[s - 1][pair], rs_send.at[pair, s - 1], rs_recv.at[j % 2, pair, s - 1])
+        for plan in rs_plan[2 * pair : 2 * pair + 2]:
+            for _, _, _, at, slot, target in plan[s - 1]:
+                to = region(j, *target)
+                g[to] = (g[to].astype(F32) + landing[at][j, slot].astype(F32)).astype(BF16)
+
     def rs_stage(j, s):
-        if s >= 1:
-            await_stage(RS_SHARDS[s - 1], rs_send.at[s - 1], rs_recv.at[j % 2, s - 1])
-        for plan in rs_plan:
+        for pair in (1, 0) if s in (2, 4) else (0, 1):
             if s >= 1:
-                for _, _, _, at, slot, target in plan[s - 1]:
-                    to = region(j, *target)
-                    g[to] = (g[to].astype(F32) + landing[at][j, slot].astype(F32)).astype(BF16)
+                rs_collect(j, s, pair)
             if s < 5:
-                for t in plan[s]:
-                    rs_start(j, s, t)
+                for plan in rs_plan[2 * pair : 2 * pair + 2]:
+                    for t in plan[s]:
+                        rs_start(j, s, pair, t)
         if s == 5:
-            rep_copy(j).start()
-
-    def rs_finish(j):
-        rep_copy(j).wait()
+            rep_copy(j, *rep_sems(j)).start()
+
+    def rs_last_ring(j):
+        for pair in (0, 1):
+            rs_collect(j, 3, pair)
+            for q in (2 * pair, 2 * pair + 1):
+                axis = ORDERS[q][0]
+                for k, by in enumerate((2, 1, -1)):
+                    pltpu.make_async_remote_copy(
+                        src_ref=g.at[region(j, q, sel_of((), axis, shifted(axis, by)), 2)], dst_ref=last_in.at[q, k],
+                        send_sem=once.at[2], recv_sem=once.at[3], device_id=peer(axis, by), device_id_type=MESH,
+                    ).start()
+
+    def rs_last_sum(j):
+        await_stage(3, once.at[2], once.at[3])
+        for q, order in enumerate(ORDERS):
+            to = region(j, q, sel_of((), order[0], own[order[0]]), 2)
+            g[to] = (g[to].astype(F32) + last_in[q, 0].astype(F32) + last_in[q, 1].astype(F32) + last_in[q, 2].astype(F32)).astype(BF16)
+        rep_copy(j, once.at[4], once.at[5]).start()
+
+    def choose(usual, for_last):
+        def stage(j):
+            if usual is not None:
+                @pl.when(j < blocks - 1)
+                def _():
+                    usual(j)
+
+            if for_last is not None:
+                @pl.when(j == blocks - 1)
+                def _():
+                    for_last(j)
+
+        return stage
+
+    def rs_finish(j, sems=rep_sems):
+        rep_copy(j, *sems(j)).wait()
         total = g[j, own["z"], own["y"], own["x"]].astype(F32) + rep_in[j].astype(F32)
         columns = pl.ds(pl.multiple_of(j * HALF, HALF), HALF)
         run[0, :, columns] = run[0, :, columns] + factor * total[:, :HALF]
@@ -211,8 +267,8 @@
         columns = pl.ds(pl.multiple_of(j * HALF, HALF), HALF)
         mine = (j, own["z"], own["y"], own["x"], ALL)
         return [
-            pltpu.make_async_copy(gw_hbm.at[:, columns], w.at[(*mine, pl.ds(0, HALF))], w_sem.at[0, j]),
-            pltpu.make_async_copy(uw_hbm.at[:, columns], w.at[(*mine, pl.ds(HALF, HALF))], w_sem.at[1, j]),
+            pltpu.make_async_copy(gw_hbm.at[:, columns], w.at[(*mine, pl.ds(0, HALF))], w_sem.at[0]),
+            pltpu.make_async_copy(uw_hbm.at[:, columns], w.at[(*mine, pl.ds(HALF, HALF))], w_sem.at[0]),
         ]
 
     @pl.loop(0, blocks)
@@ -229,10 +285,8 @@
         pl.semaphore_signal(barrier, inc=1, device_id=device, device_id_type=MESH)
     pl.semaphore_wait(barrier, len(greeted))
 
-    @pl.loop(0, blocks)
-    def _(j):
-        for c in shard_loads(j):
-            c.wait()
+    pltpu.make_async_copy(w.at[:, own["z"], own["y"], own["x"]], w.at[:, own["z"], own["y"], own["x"]], w_sem.at[0]).wait()
+    ag_first()
 
     step_rows = 32 if rows % 32 == 0 else rows
 
@@ -308,7 +362,7 @@
 
     def hidden_copy(j):
         columns = pl.ds(pl.multiple_of(j * HALF, HALF), HALF)
-        return pltpu.make_async_copy(lh.at[j], hidden_hbm.at[:, columns], out_sem.at[j])
+        return pltpu.make_async_copy(lh.at[j], hidden_hbm.at[:, columns], out_sem.at[0])
 
     def input_gradient(j):
         @pl.loop(0, 4)
@@ -350,14 +404,14 @@
         grad_copy().start()
 
     def grad_copy():
-        return pltpu.make_async_copy(dn.at[1], grad_hbm, out_sem.at[blocks])
+        return pltpu.make_async_copy(dn.at[1], grad_hbm, out_sem.at[1])
 
     def gain_copies(r):
         axis = ("x", "y", "z")[r]
         at = (own["x"], own["y"], ring_z)[r]
         return [
             pltpu.make_async_remote_copy(
-                src_ref=gbuf.at[r, at], dst_ref=gbuf.at[r, at], send_sem=gain_send.at[r, k], recv_sem=gain_recv.at[r, k],
+                src_ref=gbuf.at[r, at], dst_ref=gbuf.at[r, at], send_sem=gain_send.at[3 * r + k - 1], recv_sem=gain_recv.at[3 * r + k - 1],
                 device_id=peer(axis, k), device_id_type=MESH,
             )
             for k in (1, 2, 3)
@@ -368,7 +422,7 @@
         at = (own["x"], own["y"], ring_z)[r]
         return [
             pltpu.make_async_remote_copy(
-                src_ref=gbuf.at[r, at], dst_ref=gbuf.at[r, (at - k) % 4], send_sem=gain_send.at[r, k], recv_sem=gain_recv.at[r, k],
+                src_ref=gbuf.at[r, at], dst_ref=gbuf.at[r, (at - k) % 4], send_sem=gain_send.at[3 * r + k - 1], recv_sem=gain_recv.at[3 * r + k - 1],
                 device_id=peer(axis, k), device_id_type=MESH,
             )
             for k in (1, 2, 3)
@@ -381,7 +435,7 @@
 
     def gain_tp():
         return pltpu.make_async_remote_copy(
-            src_ref=gbuf.at[3, 0], dst_ref=gbuf.at[3, 1], send_sem=gain_send.at[3, 1], recv_sem=gain_recv.at[3, 1],
+            src_ref=gbuf.at[3, 0], dst_ref=gbuf.at[3, 1], send_sem=gain_send.at[9], recv_sem=gain_recv.at[9],
             device_id={"tp": 1 - tp}, device_id_type=MESH,
         )
 
@@ -401,9 +455,9 @@
             gain_tp().wait()
             gain_tot[...] = gain_run[...] + factor * (gbuf[3, 0] + gbuf[3, 1])
 
-    last = 5 + blocks - 1
-
-    @pl.loop(0, last + 8)
+    last = 4 + blocks - 1
+
+    @pl.loop(0, last + 6)
     def _(t):
         def at_stage(offset, run_stage):
             j = t - offset
@@ -412,24 +466,31 @@
             def _():
                 run_stage(j)
 
-        for s in (5, 4, 3, 2, 1, 0):
-            at_stage(s, functools.partial(ag_stage, s=s))
-        at_stage(11, rs_finish)
-        for s in (5, 4, 3, 2, 1):
-            at_stage(5 + s, functools.partial(rs_stage, s=s))
-
+        for s in (5, 4, 3):
+            at_stage(s - 1, functools.partial(ag_stage, s=s))
+        at_stage(1, ag_second)
+
+        @pl.when((t > 0) & (t < blocks))
+        def _():
+            ag_stage(t, 1)
+
+        @pl.when(t < blocks - 1)
+        def _():
+            ag_stage(t + 1, 0)
         for k in range(5):
             @pl.when(t == k)
             def _():
                 prepare(k)
 
-        def compute(j):
-            backward(j)
-            rs_stage(j, 0)
-            later(j)
-            input_gradient(j)
-
-        at_stage(5, compute)
+        at_stage(4, backward)
+        at_stage(10, choose(rs_finish, None))
+        at_stage(9, choose(functools.partial(rs_stage, s=5), lambda j: rs_finish(j, lambda _: (once.at[4], once.at[5]))))
+        at_stage(8, choose(functools.partial(rs_stage, s=4), rs_last_sum))
+        at_stage(7, choose(functools.partial(rs_stage, s=3), rs_last_ring))
+        for s in (2, 1, 0):
+            at_stage(4 + s, functools.partial(rs_stage, s=s))
+        at_stage(4, later)
+        at_stage(4, input_gradient)
 
         @pl.when(t == last)
         def _():
@@ -444,13 +505,38 @@
     for c in outs:
         c.start()
 
-    @pl.loop(0, blocks)
-    def _(j):
-        hidden_copy(j).wait()
-
+    pltpu.make_async_copy(lh, lh, out_sem.at[0]).wait()
     grad_copy().wait()
     for c in outs:
         c.wait()
+
+
+def copy_kernel(*refs):
+    n = (len(refs) - 2) // 3
+    sources, results, held, (into, back) = refs[:n], refs[n : 2 * n], refs[2 * n : 3 * n], refs[3 * n :]
+    reads = [pltpu.make_async_copy(a, b, into.at[i]) for i, (a, b) in enumerate(zip(sources, held))]
+    writes = [pltpu.make_async_copy(a, b, back.at[i]) for i, (a, b) in enumerate(zip(held, results))]
+    for c in reads:
+        c.start()
+    for a, b in zip(reads, writes):
+        a.wait()
+        b.start()
+    for c in writes:
+        c.wait()
+
+
+def copied(*arrays):
+    n = len(arrays)
+    hbm = pl.BlockSpec(memory_space=pl.ANY)
+    return pl.pallas_call(
+        copy_kernel,
+        out_shape=tuple(jax.ShapeDtypeStruct(a.shape, a.dtype) for a in arrays),
+        in_specs=[hbm] * n,
+        out_specs=(hbm,) * n,
+        scratch_shapes=[*[pltpu.VMEM(a.shape, a.dtype) for a in arrays], pltpu.SemaphoreType.DMA((n,)), pltpu.SemaphoreType.DMA((n,))],
+        compiler_params=pltpu.CompilerParams(vmem_limit_bytes=67043328),
+        name="hand_over",
+    )(*arrays)
 
 
 def body(later_input, earlier_input, hidden_cot, norm_gain, gate_weight, up_weight, gate_running, up_running, gain_running):
@@ -491,17 +577,19 @@
             pltpu.VMEM((2, shard, hidden), F32),
             pltpu.VMEM((4, 4, 1, width), F32),
             pltpu.VMEM((blocks, shard, 2 * HALF), BF16),
+            pltpu.VMEM((4, 3, quarter, 2 * HALF), BF16),
             *[pltpu.VMEM(s, BF16) for s in landing_shapes(blocks, quarter)],
+            dma((2, 5)),
+            dma((2, 2, 5)),
+            dma((2, 6)),
+            dma((2, 2, 6)),
+            dma((6,)),
             dma((5,)),
-            dma((2, 5)),
-            dma((6,)),
-            dma((2, 6)),
-            dma((5,)),
-            dma((2, blocks)),
+            dma((1,)),
             dma((4,)),
             dma((4,)),
-            dma((2, 4, 4)),
-            dma((blocks + 1,)),
+            dma((2, 10)),
+            dma((2,)),
         ],
         compiler_params=pltpu.CompilerParams(collective_id=0, has_side_effects=True, vmem_limit_bytes=67043328),
         cost_estimate=pl.CostEstimate(flops=16 * rows * width * hidden * 2, bytes_accessed=16 << 20, transcendentals=0),
@@ -510,7 +598,7 @@
         later_input, earlier_input, hidden_cot, norm_gain.reshape(1, width), gate_weight, up_weight, gate_running, up_running,
         gain_running.reshape(1, width),
     )
-    hidden_out, grad, gate_total, up_total, gain_total = out
+    hidden_out, grad, gate_total, up_total, gain_total = copied(*out)
     return hidden_out, grad, gate_total, up_total, gain_total.reshape(width)
 
 

time: 142 us -> 124 us (0.87)
  Pallas kernels: 136 us -> 123 us
  local copies, waits for them, and re-layouts: 5.9 us -> 0 us
    pallas_call x1, Pallas kernels: 136 us -> 120 us  [body(): pl.pallas_call(functools.partial(kernel, blocks, factor), out_shape=(jax....]
    unnamed x13 -> x0, local copies, waits for them, and re-layouts: 5.9 us -> none
    pallas_call x0 -> x1, Pallas kernels: none -> 3.13 us  [copied(): pl.pallas_call(copy_kernel, out_shape=tuple((jax.ShapeDtypeStruct(a.shape...]
where the time goes in v3:
time: 124 us
  Pallas kernels  123 us (99%)
    pallas_call x1, Pallas kernels, body(): pl.pallas_call(functools.partial(kernel, blocks, factor), out_shape=(jax....  120 us
    pallas_call x1, Pallas kernels, copied(): pl.pallas_call(copy_kernel, out_shape=tuple((jax.ShapeDtypeStruct(a.shape...  3.13 us

profile of v3, /device:TPU:0, one launch (start us, length us, event | category | flops | bytes accessed | tf_op | source)
XLA Modules:
  0.0 123.5 jit_solution(18409046760508212458)
XLA Ops:
  0.6 119.7 %half_step.1 = (bf16[512,1408]{1,0:T(8,128)(2,1)}, bf16[256,2048]{1,0:T(8,128)(2,1)}, f32[64,1408]{1,0:T(8,128)}, f32[64,1408]{1,0:T(8,128)}, f32[1,2048]{1,0:T(1,128)}) custom-call(bf16[256,2048]{1,0:T(8,128)(2,1)} %later_hbm.1, bf16[256,2048]{1,0:T(8,128)(2,1)} %earlier_hbm.1, bf16[512,1408]{1,0:T(8,128)(2,1)} %cot_hbm.1, f32[1,2048]{1,0:T(1,128)} %bitcast.3, ...), custom_call_target="tpu_custom_call" | custom-call | flops 23622320128 | bytes 16777216 | tf_op jit(solution)/shard_map/half_step/pallas_call | solution.py:553
  120.4 3.1 %hand_over.1 = (bf16[512,1408]{1,0:T(8,128)(2,1)}, bf16[256,2048]{1,0:T(8,128)(2,1)}, f32[64,1408]{1,0:T(8,128)}, f32[64,1408]{1,0:T(8,128)}, f32[1,2048]{1,0:T(1,128)}) custom-call(bf16[512,1408]{1,0:T(8,128)(2,1)} %get-tuple-element.15.refs_0_, bf16[256,2048]{1,0:T(8,128)(2,1)} %get-tuple-element.16.refs_1_, f32[64,1408]{1,0:T(8,128)} %get-tuple-element.17.refs_2_, ...), custom_call_target="tpu_custom_call" | custom-call | tf_op jit(solution)/shard_map/hand_over/pallas_call | solution.py:531

commit v4 on v3

--- a/solution.py
+++ b/solution.py
@@ -14,6 +14,7 @@
 F32, BF16 = jnp.float32, jnp.bfloat16
 SIZE = {"z": 2, "y": 4, "x": 4}
 ORDERS = (("y", "z", "x"), ("x", "z", "y"), ("x", "y", "z"), ("y", "x", "z"))
+ORDERS_MID = ORDERS[:2] + (("x", "z", "y"), ("y", "z", "x"))
 ALL = slice(None)
 AG_SHARDS = ((1, 1), (0.5, 0.5), (2, 4), (8, 2), (4, 8))
 RS_SHARDS = ((4, 8), (8, 2), (2, 4), (0.5, 0.5), (1, 1))
@@ -23,9 +24,9 @@
     return 1.0 / (1.0 + jnp.exp(-v))
 
 
-def landing_shapes(blocks, quarter):
+def landing_shapes(orders, blocks, quarter):
     shapes = []
-    for order in ORDERS:
+    for order in orders:
         full = [a for a in "zyx"]
         for axis in reversed(order):
             full.remove(axis)
@@ -43,8 +44,8 @@
     hidden_hbm, grad_hbm, gtot_hbm, utot_hbm, gain_tot,
     w, g, xin, xl, xe, xt, cot, d, acc, lh, dn, inv_ref, run, gbuf, rep_in, *rest,
 ):
-    last_in, landing = rest[0], list(rest[1:-11])
-    ag_send, ag_recv, rs_send, rs_recv, once, load_sem, w_sem, tp_send, tp_recv, gs, out_sem = rest[-11:]
+    last_in, landing = rest[0], list(rest[1:-12])
+    ag_send, ag_recv, early, rs_send, rs_recv, once, load_sem, w_sem, tp_send, tp_recv, gs, out_sem = rest[-12:]
     gain_send, gain_recv = gs.at[0], gs.at[1]
     rows = xin.shape[1]
     width = xin.shape[2]
@@ -75,28 +76,32 @@
         s[axis] = coordinate
         return s
 
-    ag_plan = []
-    count = 0
-    for q, order in enumerate(ORDERS):
-        phases = []
-        for p, axis in enumerate(order):
-            full = order[:p]
-            if axis == "z":
-                group = []
-                for k, by in enumerate((1, -1)):
-                    group.append((count, (q, sel_of(full, "z", own["z"]), k), ("z", by), (q, sel_of(full, "z", 1 - own["z"]), k)))
-                    count += 1
-                phases.append(("z", [group]))
-            else:
-                first, second = [], []
-                for k, by in enumerate((1, -1)):
-                    first.append((count, (q, sel_of(full, axis, own[axis]), 2), (axis, by), (q, sel_of(full, axis, shifted(axis, -by)), 2)))
-                    count += 1
-                for k, by in enumerate((1, -1)):
-                    second.append((count, (q, sel_of(full, axis, shifted(axis, -by)), k), (axis, by), (q, sel_of(full, axis, shifted(axis, 2)), k)))
-                    count += 1
-                phases.append((axis, [first, second]))
-        ag_plan.append([group for _, groups in phases for group in groups])
+    def plan_gather(orders):
+        plans, count = [], 0
+        for q, order in enumerate(orders):
+            phases = []
+            for p, axis in enumerate(order):
+                full = order[:p]
+                if axis == "z":
+                    group = []
+                    for k, by in enumerate((1, -1)):
+                        group.append((count, (q, sel_of(full, "z", own["z"]), k), ("z", by), (q, sel_of(full, "z", 1 - own["z"]), k)))
+                        count += 1
+                    phases.append(("z", [group]))
+                else:
+                    first, second = [], []
+                    for k, by in enumerate((1, -1)):
+                        first.append((count, (q, sel_of(full, axis, own[axis]), 2), (axis, by), (q, sel_of(full, axis, shifted(axis, -by)), 2)))
+                        count += 1
+                    for k, by in enumerate((1, -1)):
+                        second.append((count, (q, sel_of(full, axis, shifted(axis, -by)), k), (axis, by), (q, sel_of(full, axis, shifted(axis, 2)), k)))
+                        count += 1
+                    phases.append((axis, [first, second]))
+            plans.append([group for _, groups in phases for group in groups])
+        return plans
+
+    ag_plans = plan_gather(ORDERS), plan_gather(ORDERS_MID)
+    ag_plan = ag_plans[0]
 
     def shards(n):
         if n <= 4:
@@ -116,14 +121,32 @@
             src_ref=w.at[region(j, *src)], dst_ref=w.at[region(j, *src)], send_sem=send, recv_sem=recv, device_id=peer(*to), device_id_type=MESH
         ).start()
 
+    middle = blocks // 2
+
+    def per_kind(j, pair, run):
+        if pair == 0:
+            run(0)
+            return
+
+        @pl.when(j != middle)
+        def _():
+            run(0)
+
+        @pl.when(j == middle)
+        def _():
+            run(1)
+
     def ag_stage(j, s, wait=True):
         for pair in (1, 0):
-            if s >= 1 and wait:
-                await_stage(AG_SHARDS[s - 1][pair], ag_send.at[pair, s - 1], ag_recv.at[j % 2, pair, s - 1])
-            if s < 5:
-                for plan in ag_plan[2 * pair : 2 * pair + 2]:
-                    for _, src, to, _ in plan[s]:
-                        ag_send_to(j, src, to, ag_send.at[pair, s], ag_recv.at[j % 2, pair, s])
+            def part(kind):
+                if wait:
+                    await_stage(AG_SHARDS[s - 1][0 if kind else pair], ag_send.at[pair + kind, s - 3], ag_recv.at[j % 3, pair + kind, s - 3])
+                if s < 5:
+                    for plan in ag_plans[kind][2 * pair : 2 * pair + 2]:
+                        for _, src, to, _ in plan[s]:
+                            ag_send_to(j, src, to, ag_send.at[pair + kind, s - 2], ag_recv.at[j % 3, pair + kind, s - 2])
+
+            per_kind(j, pair, part)
 
     def ag_first():
         for q, order in enumerate(ORDERS):
@@ -131,47 +154,70 @@
             for by in (2, 1, -1):
                 ag_send_to(0, src, (order[0], by), once.at[0], once.at[1])
 
+    groups = (pl.ds(1, 1), pl.ds(2, blocks - 2))
+
+    def ag_early(s, k):
+        if s == 1:
+            await_early(0, k)
+        for plan in ag_plan:
+            for _, src, to, _ in plan[s]:
+                ag_send_to(groups[k], src, to, early.at[k, 0, s], early.at[k, 1, s])
+
+    def await_early(s, k):
+        for way in (0, 1):
+            view = w.at[groups[k], 0, 0, pl.ds(0, 2)] if s == 0 else w.at[groups[k], 0, 0, 0]
+            pltpu.make_async_copy(view, view, early.at[k, way, s]).wait()
+
     def ag_second(j):
         @pl.when(j == 0)
         def _():
             await_stage(3, once.at[0], once.at[1])
-            ag_stage(j, 2, wait=False)
-
-        @pl.when(j > 0)
-        def _():
-            ag_stage(j, 2)
-
-    rs_plan = []
-    count, place = 0, 0
-    for q, order in enumerate(ORDERS):
-        groups = []
-        full = ["z", "y", "x"]
-        for axis in reversed(order):
-            full.remove(axis)
-            if axis == "z":
-                group = []
-                for k, by in enumerate((1, -1)):
-                    group.append((count, (q, sel_of(full, "z", 1 - own["z"]), k), ("z", by), place, k, (q, sel_of(full, "z", own["z"]), k)))
-                    count += 1
-                groups.append(group)
-                place += 1
-            else:
-                first, second = [], []
-                for k, by in enumerate((1, -1)):
-                    first.append((count, (q, sel_of(full, axis, shifted(axis, 2)), k), (axis, by), place, k, (q, sel_of(full, axis, shifted(axis, by)), k)))
-                    count += 1
-                for k, by in enumerate((1, -1)):
-                    second.append((count, (q, sel_of(full, axis, shifted(axis, by)), 2), (axis, by), place + 1, k, (q, sel_of(full, axis, own[axis]), 2)))
-                    count += 1
-                groups += [first, second]
-                place += 2
-        rs_plan.append(groups)
-
-    def rs_start(j, s, pair, t):
+
+        for k in (0, 1):
+            @pl.when(j == 1 + k)
+            def _():
+                await_early(1, k)
+
+        ag_stage(j, 2, wait=False)
+
+    def plan_scatter(orders, place):
+        plans, count = [], 0
+        for q, order in enumerate(orders):
+            groups = []
+            full = ["z", "y", "x"]
+            for axis in reversed(order):
+                full.remove(axis)
+                if axis == "z":
+                    group = []
+                    for k, by in enumerate((1, -1)):
+                        group.append((count, (q, sel_of(full, "z", 1 - own["z"]), k), ("z", by), place, k, (q, sel_of(full, "z", own["z"]), k)))
+                        count += 1
+                    groups.append(group)
+                    place += 1
+                else:
+                    first, second = [], []
+                    for k, by in enumerate((1, -1)):
+                        first.append((count, (q, sel_of(full, axis, shifted(axis, 2)), k), (axis, by), place, k, (q, sel_of(full, axis, shifted(axis, by)), k)))
+                        count += 1
+                    for k, by in enumerate((1, -1)):
+                        second.append((count, (q, sel_of(full, axis, shifted(axis, by)), 2), (axis, by), place + 1, k, (q, sel_of(full, axis, own[axis]), 2)))
+                        count += 1
+                    groups += [first, second]
+                    place += 2
+            plans.append(groups)
+        return plans
+
+    half_landing = len(landing) // 2
+    rs_plans = plan_scatter(ORDERS, 0), plan_scatter(ORDERS_MID, half_landing)
+
+    def land(kind, j, at, slot):
+        return landing[at].at[0 if kind else j, slot]
+
+    def rs_start(j, s, pair, kind, t):
         _, src, to, at, slot, _ = t
         pltpu.make_async_remote_copy(
-            src_ref=g.at[region(j, *src)], dst_ref=landing[at].at[j, slot], send_sem=rs_send.at[pair, s], recv_sem=rs_recv.at[j % 2, pair, s],
-            device_id=peer(*to), device_id_type=MESH,
+            src_ref=g.at[region(j, *src)], dst_ref=land(kind, j, at, slot), send_sem=rs_send.at[pair + kind, s],
+            recv_sem=rs_recv.at[j % 3, pair + kind, s], device_id=peer(*to), device_id_type=MESH,
         ).start()
 
     def rep_copy(j, send, recv):
@@ -181,23 +227,26 @@
         )
 
     def rep_sems(j):
-        return rs_send.at[0, 5], rs_recv.at[j % 2, 0, 5]
-
-    def rs_collect(j, s, pair):
-        await_stage(RS_SHARDS[s - 1][pair], rs_send.at[pair, s - 1], rs_recv.at[j % 2, pair, s - 1])
-        for plan in rs_plan[2 * pair : 2 * pair + 2]:
+        return rs_send.at[0, 5], rs_recv.at[j % 3, 0, 5]
+
+    def rs_collect(j, s, pair, kind=0):
+        await_stage(RS_SHARDS[s - 1][0 if kind else pair], rs_send.at[pair + kind, s - 1], rs_recv.at[j % 3, pair + kind, s - 1])
+        for plan in rs_plans[kind][2 * pair : 2 * pair + 2]:
             for _, _, _, at, slot, target in plan[s - 1]:
                 to = region(j, *target)
-                g[to] = (g[to].astype(F32) + landing[at][j, slot].astype(F32)).astype(BF16)
+                g[to] = (g[to].astype(F32) + land(kind, j, at, slot)[...].astype(F32)).astype(BF16)
 
     def rs_stage(j, s):
         for pair in (1, 0) if s in (2, 4) else (0, 1):
-            if s >= 1:
-                rs_collect(j, s, pair)
-            if s < 5:
-                for plan in rs_plan[2 * pair : 2 * pair + 2]:
-                    for t in plan[s]:
-                        rs_start(j, s, pair, t)
+            def part(kind):
+                if s >= 1:
+                    rs_collect(j, s, pair, kind)
+                if s < 5:
+                    for plan in rs_plans[kind][2 * pair : 2 * pair + 2]:
+                        for t in plan[s]:
+                            rs_start(j, s, pair, kind, t)
+
+            per_kind(j, pair, part)
         if s == 5:
             rep_copy(j, *rep_sems(j)).start()
 
@@ -239,6 +288,8 @@
         columns = pl.ds(pl.multiple_of(j * HALF, HALF), HALF)
         run[0, :, columns] = run[0, :, columns] + factor * total[:, :HALF]
         run[1, :, columns] = run[1, :, columns] + factor * total[:, HALF:]
+        pltpu.make_async_copy(run.at[0, :, columns], gtot_hbm.at[:, columns], out_sem.at[2]).start()
+        pltpu.make_async_copy(run.at[1, :, columns], utot_hbm.at[:, columns], out_sem.at[2]).start()
 
     def tp_copy(i, ref):
         return pltpu.make_async_remote_copy(
@@ -287,6 +338,8 @@
 
     pltpu.make_async_copy(w.at[:, own["z"], own["y"], own["x"]], w.at[:, own["z"], own["y"], own["x"]], w_sem.at[0]).wait()
     ag_first()
+    ag_early(0, 0)
+    ag_early(0, 1)
 
     step_rows = 32 if rows % 32 == 0 else rows
 
@@ -307,14 +360,14 @@
             normalize(1, xe)
             tp_copy(1, xe.at[tp]).start()
         elif t == 1:
-            slab = min(256, width)
+            slab, mine = min(256, width), pl.ds(pl.multiple_of(tp * rows, rows), rows)
 
             @pl.loop(0, width // slab)
             def _(i):
                 at = pl.ds(pl.multiple_of(i * slab, slab), slab)
-                xt[tp, at, :] = xe[tp, :, at].T
-
-            tp_copy(2, xt.at[tp]).start()
+                xt[at, mine] = xe[tp, :, at].T
+
+            tp_copy(2, xt.at[:, mine]).start()
         elif t == 2:
             normalize(0, xl)
             tp_copy(0, xl.at[tp]).start()
@@ -324,9 +377,11 @@
             exchanged()
 
     def exchanged():
-        for i, ref in ((0, xl), (1, xe), (2, xt)):
+        for i, ref in ((0, xl), (1, xe)):
             tp_copy(i, ref.at[tp]).wait_send()
             tp_received(i, ref.at[1 - tp]).wait_recv()
+        tp_copy(2, xt.at[:, pl.ds(pl.multiple_of(tp * rows, rows), rows)]).wait_send()
+        tp_received(2, xt.at[:, pl.ds(pl.multiple_of((1 - tp) * rows, rows), rows)]).wait_recv()
 
     def block_weight(j):
         return w[j].reshape(width, 2 * HALF)
@@ -347,8 +402,7 @@
         def _(k):
             z, y = k // 2, 2 * (k % 2)
             at = pl.ds(pl.multiple_of(k * (width // 4), width // 4), width // 4)
-            part = jnp.dot(xt[0, at, :], d[0], preferred_element_type=F32)
-            part = part + jnp.dot(xt[1, at, :], d[1], preferred_element_type=F32)
+            part = jnp.dot(xt[at, :], d[...].reshape(2 * rows, 2 * HALF), preferred_element_type=F32)
             g[j, z, pl.ds(y, 2)] = part.astype(BF16).reshape(2, 4, 4 * quarter, 2 * HALF)
 
     def later(j):
@@ -470,13 +524,10 @@
             at_stage(s - 1, functools.partial(ag_stage, s=s))
         at_stage(1, ag_second)
 
-        @pl.when((t > 0) & (t < blocks))
-        def _():
-            ag_stage(t, 1)
-
-        @pl.when(t < blocks - 1)
-        def _():
-            ag_stage(t + 1, 0)
+        for k in (0, 1):
+            @pl.when(t == 1 + k)
+            def _():
+                ag_early(1, k)
         for k in range(5):
             @pl.when(t == k)
             def _():
@@ -487,8 +538,9 @@
         at_stage(9, choose(functools.partial(rs_stage, s=5), lambda j: rs_finish(j, lambda _: (once.at[4], once.at[5]))))
         at_stage(8, choose(functools.partial(rs_stage, s=4), rs_last_sum))
         at_stage(7, choose(functools.partial(rs_stage, s=3), rs_last_ring))
-        for s in (2, 1, 0):
-            at_stage(4 + s, functools.partial(rs_stage, s=s))
+        at_stage(6, functools.partial(rs_stage, s=2))
+        at_stage(5, functools.partial(rs_stage, s=1))
+        at_stage(4, functools.partial(rs_stage, s=0))
         at_stage(4, later)
         at_stage(4, input_gradient)
 
@@ -501,14 +553,9 @@
             def _():
                 gain_step(r)
 
-    outs = [pltpu.make_async_copy(run.at[0], gtot_hbm, load_sem.at[0]), pltpu.make_async_copy(run.at[1], utot_hbm, load_sem.at[1])]
-    for c in outs:
-        c.start()
-
     pltpu.make_async_copy(lh, lh, out_sem.at[0]).wait()
     grad_copy().wait()
-    for c in outs:
-        c.wait()
+    pltpu.make_async_copy(run, run, out_sem.at[2]).wait()
 
 
 def copy_kernel(*refs):
@@ -567,7 +614,7 @@
             pltpu.VMEM((2, rows, width), BF16),
             pltpu.VMEM((2, rows, width), BF16),
             pltpu.VMEM((2, rows, width), BF16),
-            pltpu.VMEM((2, width, rows), BF16),
+            pltpu.VMEM((width, 2 * rows), BF16),
             pltpu.VMEM((2 * rows, hidden), BF16),
             pltpu.VMEM((2, rows, 2 * HALF), BF16),
             pltpu.VMEM((2, rows, width), F32),
@@ -578,18 +625,20 @@
             pltpu.VMEM((4, 4, 1, width), F32),
             pltpu.VMEM((blocks, shard, 2 * HALF), BF16),
             pltpu.VMEM((4, 3, quarter, 2 * HALF), BF16),
-            *[pltpu.VMEM(s, BF16) for s in landing_shapes(blocks, quarter)],
-            dma((2, 5)),
-            dma((2, 2, 5)),
-            dma((2, 6)),
-            dma((2, 2, 6)),
+            *[pltpu.VMEM(s, BF16) for s in landing_shapes(ORDERS, blocks, quarter)],
+            *[pltpu.VMEM(s, BF16) for s in landing_shapes(ORDERS_MID, 1, quarter)],
+            dma((3, 3)),
+            dma((3, 3, 3)),
+            dma((2, 2, 2)),
+            dma((3, 6)),
+            dma((3, 3, 6)),
             dma((6,)),
             dma((5,)),
             dma((1,)),
             dma((4,)),
             dma((4,)),
             dma((2, 10)),
-            dma((2,)),
+            dma((3,)),
         ],
         compiler_params=pltpu.CompilerParams(collective_id=0, has_side_effects=True, vmem_limit_bytes=67043328),
         cost_estimate=pl.CostEstimate(flops=16 * rows * width * hidden * 2, bytes_accessed=16 << 20, transcendentals=0),

time: 124 us -> 121 us (0.976)
  Pallas kernels: 123 us -> 120 us
    pallas_call x1, Pallas kernels: 120 us -> 117 us  [body(): pl.pallas_call(functools.partial(kernel, blocks, factor), out_shape=(jax....]
where the time goes in v4:
time: 121 us
  Pallas kernels  120 us (99%)
    pallas_call x1, Pallas kernels, body(): pl.pallas_call(functools.partial(kernel, blocks, factor), out_shape=(jax....  117 us
    pallas_call x1, Pallas kernels, copied(): pl.pallas_call(copy_kernel, out_shape=tuple((jax.ShapeDtypeStruct(a.shape...  3.13 us

profile of v4, /device:TPU:0, one launch (start us, length us, event | category | flops | bytes accessed | tf_op | source)
XLA Modules:
  0.0 121.1 jit_solution(10402039485781592408)
XLA Ops:
  0.6 117.3 %half_step.1 = (bf16[512,1408]{1,0:T(8,128)(2,1)}, bf16[256,2048]{1,0:T(8,128)(2,1)}, f32[64,1408]{1,0:T(8,128)}, f32[64,1408]{1,0:T(8,128)}, f32[1,2048]{1,0:T(1,128)}) custom-call(bf16[256,2048]{1,0:T(8,128)(2,1)} %later_hbm.1, bf16[256,2048]{1,0:T(8,128)(2,1)} %earlier_hbm.1, bf16[512,1408]{1,0:T(8,128)(2,1)} %cot_hbm.1, f32[1,2048]{1,0:T(1,128)} %bitcast.3, ...), custom_call_target="tpu_custom_call" | custom-call | flops 23622320128 | bytes 16777216 | tf_op jit(solution)/shard_map/half_step/pallas_call | solution.py:600
  117.9 3.1 %hand_over.1 = (bf16[512,1408]{1,0:T(8,128)(2,1)}, bf16[256,2048]{1,0:T(8,128)(2,1)}, f32[64,1408]{1,0:T(8,128)}, f32[64,1408]{1,0:T(8,128)}, f32[1,2048]{1,0:T(1,128)}) custom-call(bf16[512,1408]{1,0:T(8,128)(2,1)} %get-tuple-element.15.refs_0_, bf16[256,2048]{1,0:T(8,128)(2,1)} %get-tuple-element.16.refs_1_, f32[64,1408]{1,0:T(8,128)} %get-tuple-element.17.refs_2_, ...), custom_call_target="tpu_custom_call" | custom-call | tf_op jit(solution)/shard_map/hand_over/pallas_call | solution.py:578

commit v5 on v4

--- a/solution.py
+++ b/solution.py
@@ -41,11 +41,11 @@
 
 def kernel(
     blocks, factor, later_hbm, earlier_hbm, cot_hbm, gain_ref, gw_hbm, uw_hbm, grun_hbm, urun_hbm, gain_run,
-    hidden_hbm, grad_hbm, gtot_hbm, utot_hbm, gain_tot,
-    w, g, xin, xl, xe, xt, cot, d, acc, lh, dn, inv_ref, run, gbuf, rep_in, *rest,
+    hidden_out, grad_out, gtot_out, utot_out, gain_tot,
+    w, g, xin, xl, xe, xt, cot, d, acc, dn, inv_ref, run, gbuf, rep_in, *rest,
 ):
-    last_in, landing = rest[0], list(rest[1:-12])
-    ag_send, ag_recv, early, rs_send, rs_recv, once, load_sem, w_sem, tp_send, tp_recv, gs, out_sem = rest[-12:]
+    last_in, landing = rest[0], list(rest[1:-11])
+    ag_send, ag_recv, early, rs_send, rs_recv, once, load_sem, w_sem, tp_send, tp_recv, gs = rest[-11:]
     gain_send, gain_recv = gs.at[0], gs.at[1]
     rows = xin.shape[1]
     width = xin.shape[2]
@@ -286,10 +286,8 @@
         rep_copy(j, *sems(j)).wait()
         total = g[j, own["z"], own["y"], own["x"]].astype(F32) + rep_in[j].astype(F32)
         columns = pl.ds(pl.multiple_of(j * HALF, HALF), HALF)
-        run[0, :, columns] = run[0, :, columns] + factor * total[:, :HALF]
-        run[1, :, columns] = run[1, :, columns] + factor * total[:, HALF:]
-        pltpu.make_async_copy(run.at[0, :, columns], gtot_hbm.at[:, columns], out_sem.at[2]).start()
-        pltpu.make_async_copy(run.at[1, :, columns], utot_hbm.at[:, columns], out_sem.at[2]).start()
+        gtot_out[:, columns] = run[0, :, columns] + factor * total[:, :HALF]
+        utot_out[:, columns] = run[1, :, columns] + factor * total[:, HALF:]
 
     def tp_copy(i, ref):
         return pltpu.make_async_remote_copy(
@@ -389,34 +387,28 @@
     def backward(j):
         columns = pl.ds(pl.multiple_of(j * HALF, HALF), HALF)
 
-        @pl.loop(0, 2)
-        def _(m):
+        for m in range(2):
             both = jnp.dot(xe[m], block_weight(j), preferred_element_type=F32)
             gate, up = both[:, :HALF], both[:, HALF:]
             s = sigmoid(gate)
-            c = cot[pl.ds(pl.multiple_of(m * rows, rows), rows), columns].astype(F32)
+            c = cot[pl.ds(m * rows, rows), columns].astype(F32)
             d[m, :, 0:HALF] = (c * up * s * (1.0 + gate * (1.0 - s))).astype(BF16)
             d[m, :, HALF:] = (c * gate * s).astype(BF16)
 
-        @pl.loop(0, 4)
-        def _(k):
+        for k in range(4):
             z, y = k // 2, 2 * (k % 2)
-            at = pl.ds(pl.multiple_of(k * (width // 4), width // 4), width // 4)
+            at = pl.ds(k * (width // 4), width // 4)
             part = jnp.dot(xt[at, :], d[...].reshape(2 * rows, 2 * HALF), preferred_element_type=F32)
             g[j, z, pl.ds(y, 2)] = part.astype(BF16).reshape(2, 4, 4 * quarter, 2 * HALF)
 
     def later(j):
+        columns = pl.ds(pl.multiple_of(j * HALF, HALF), HALF)
+
         @pl.loop(0, 2)
         def _(m):
             both = jnp.dot(xl[m], block_weight(j), preferred_element_type=F32)
             gate, up = both[:, :HALF], both[:, HALF:]
-            lh[j, pl.ds(pl.multiple_of(m * rows, rows), rows), :] = (gate * sigmoid(gate) * up).astype(BF16)
-
-        hidden_copy(j).start()
-
-    def hidden_copy(j):
-        columns = pl.ds(pl.multiple_of(j * HALF, HALF), HALF)
-        return pltpu.make_async_copy(lh.at[j], hidden_hbm.at[:, columns], out_sem.at[0])
+            hidden_out[pl.ds(pl.multiple_of(m * rows, rows), rows), columns] = (gate * sigmoid(gate) * up).astype(BF16)
 
     def input_gradient(j):
         @pl.loop(0, 4)
@@ -452,13 +444,8 @@
             inv = inv_ref[at, :]
             scaled = d_norm * gain
             inner = jnp.mean(scaled * values, axis=1, keepdims=True)
-            dn[1, at, :] = (inv * scaled - values * (inv * inv * inv) * inner).astype(BF16)
+            grad_out[at, :] = (inv * scaled - values * (inv * inv * inv) * inner).astype(BF16)
             own_slot[...] = own_slot[...] + jnp.sum(d_norm * values * inv, axis=0, keepdims=True)
-
-        grad_copy().start()
-
-    def grad_copy():
-        return pltpu.make_async_copy(dn.at[1], grad_hbm, out_sem.at[1])
 
     def gain_copies(r):
         axis = ("x", "y", "z")[r]
@@ -553,35 +540,25 @@
             def _():
                 gain_step(r)
 
-    pltpu.make_async_copy(lh, lh, out_sem.at[0]).wait()
-    grad_copy().wait()
-    pltpu.make_async_copy(run, run, out_sem.at[2]).wait()
-
 
 def copy_kernel(*refs):
-    n = (len(refs) - 2) // 3
-    sources, results, held, (into, back) = refs[:n], refs[n : 2 * n], refs[2 * n : 3 * n], refs[3 * n :]
-    reads = [pltpu.make_async_copy(a, b, into.at[i]) for i, (a, b) in enumerate(zip(sources, held))]
-    writes = [pltpu.make_async_copy(a, b, back.at[i]) for i, (a, b) in enumerate(zip(held, results))]
-    for c in reads:
+    n = len(refs) // 2
+    copies = [pltpu.make_async_copy(a, b, refs[-1].at[i]) for i, (a, b) in enumerate(zip(refs[:n], refs[n : 2 * n]))]
+    for c in copies:
         c.start()
-    for a, b in zip(reads, writes):
-        a.wait()
-        b.start()
-    for c in writes:
+    for c in copies:
         c.wait()
 
 
 def copied(*arrays):
     n = len(arrays)
-    hbm = pl.BlockSpec(memory_space=pl.ANY)
     return pl.pallas_call(
         copy_kernel,
         out_shape=tuple(jax.ShapeDtypeStruct(a.shape, a.dtype) for a in arrays),
-        in_specs=[hbm] * n,
-        out_specs=(hbm,) * n,
-        scratch_shapes=[*[pltpu.VMEM(a.shape, a.dtype) for a in arrays], pltpu.SemaphoreType.DMA((n,)), pltpu.SemaphoreType.DMA((n,))],
-        compiler_params=pltpu.CompilerParams(vmem_limit_bytes=67043328),
+        in_specs=[pl.BlockSpec(memory_space=pltpu.VMEM)] * n,
+        out_specs=(pl.BlockSpec(memory_space=pl.ANY),) * n,
+        scratch_shapes=[pltpu.SemaphoreType.DMA((n,))],
+        compiler_params=pltpu.CompilerParams(vmem_limit_bytes=16 << 20),
         name="hand_over",
     )(*arrays)
 
@@ -600,14 +577,14 @@
     out = pl.pallas_call(
         functools.partial(kernel, blocks, factor),
         out_shape=(
-            jax.ShapeDtypeStruct((2 * rows, hidden), BF16),
-            jax.ShapeDtypeStruct((rows, width), BF16),
-            jax.ShapeDtypeStruct((shard, hidden), F32),
-            jax.ShapeDtypeStruct((shard, hidden), F32),
-            jax.ShapeDtypeStruct((1, width), F32),
+            pltpu.VMEM((2 * rows, hidden), BF16),
+            pltpu.VMEM((rows, width), BF16),
+            pltpu.VMEM((shard, hidden), F32),
+            pltpu.VMEM((shard, hidden), F32),
+            pltpu.VMEM((1, width), F32),
         ),
         in_specs=[hbm, hbm, hbm, vmem, hbm, hbm, hbm, hbm, vmem],
-        out_specs=(hbm, hbm, hbm, hbm, vmem),
+        out_specs=(vmem, vmem, vmem, vmem, vmem),
         scratch_shapes=[
             pltpu.VMEM(whole, BF16),
             pltpu.VMEM(whole, BF16),
@@ -618,7 +595,6 @@
             pltpu.VMEM((2 * rows, hidden), BF16),
             pltpu.VMEM((2, rows, 2 * HALF), BF16),
             pltpu.VMEM((2, rows, width), F32),
-            pltpu.VMEM((blocks, 2 * rows, HALF), BF16),
             pltpu.VMEM((3, rows, width), BF16),
             pltpu.VMEM((rows, 1), F32),
             pltpu.VMEM((2, shard, hidden), F32),
@@ -638,9 +614,8 @@
             dma((4,)),
             dma((4,)),
             dma((2, 10)),
-            dma((3,)),
         ],
-        compiler_params=pltpu.CompilerParams(collective_id=0, has_side_effects=True, vmem_limit_bytes=67043328),
+        compiler_params=pltpu.CompilerParams(collective_id=0, has_side_effects=True, vmem_limit_bytes=58 << 20),
         cost_estimate=pl.CostEstimate(flops=16 * rows * width * hidden * 2, bytes_accessed=16 << 20, transcendentals=0),
         name="half_step",
     )(

time: 121 us -> 118 us (0.975)
  Pallas kernels: 120 us -> 118 us
    pallas_call x1, Pallas kernels: 117 us -> 116 us  [body(): pl.pallas_call(functools.partial(kernel, blocks, factor), out_shape=(pltp...]
    pallas_call x1, Pallas kernels: 3.13 us -> 1.72 us  [copied(): pl.pallas_call(copy_kernel, out_shape=tuple((jax.ShapeDtypeStruct(a.shape...]
where the time goes in v5:
time: 118 us
  Pallas kernels  118 us (100%)
    pallas_call x1, Pallas kernels, body(): pl.pallas_call(functools.partial(kernel, blocks, factor), out_shape=(pltp...  116 us

profile of v5, /device:TPU:0, one launch (start us, length us, event | category | flops | bytes accessed | tf_op | source)
XLA Modules:
  0.0 118.2 jit_solution(14347836023525203034)
XLA Ops:
  0.6 115.8 %half_step.1 = (bf16[512,1408]{1,0:T(8,128)(2,1)S(1)}, bf16[256,2048]{1,0:T(8,128)(2,1)S(1)}, f32[64,1408]{1,0:T(8,128)S(1)}, f32[64,1408]{1,0:T(8,128)S(1)}, f32[1,2048]{1,0:T(1,128)S(1)}) custom-call(bf16[256,2048]{1,0:T(8,128)(2,1)} %later_hbm.1, bf16[256,2048]{1,0:T(8,128)(2,1)} %earlier_hbm.1, bf16[512,1408]{1,0:T(8,128)(2,1)} %cot_hbm.1, ...), custom_call_target="tpu_custom_call" | custom-call | flops 23622320128 | bytes 16777216 | tf_op jit(solution)/shard_map/half_step/pallas_call | solution.py:577
  116.4 1.7 %hand_over.1 = (bf16[512,1408]{1,0:T(8,128)(2,1)}, bf16[256,2048]{1,0:T(8,128)(2,1)}, f32[64,1408]{1,0:T(8,128)}, f32[64,1408]{1,0:T(8,128)}, f32[1,2048]{1,0:T(1,128)}) custom-call(bf16[512,1408]{1,0:T(8,128)(2,1)S(1)} %get-tuple-element.15.refs_0_, bf16[256,2048]{1,0:T(8,128)(2,1)S(1)} %get-tuple-element.16.refs_1_, ...), custom_call_target="tpu_custom_call" | custom-call | tf_op jit(solution)/shard_map/hand_over/pallas_call | solution.py:555

commit v6 on v5

--- a/solution.py
+++ b/solution.py
@@ -511,14 +511,15 @@
             at_stage(s - 1, functools.partial(ag_stage, s=s))
         at_stage(1, ag_second)
 
-        for k in (0, 1):
-            @pl.when(t == 1 + k)
-            def _():
-                ag_early(1, k)
+        @pl.when(t == 1)
+        def _():
+            ag_early(1, 0)
         for k in range(5):
             @pl.when(t == k)
             def _():
                 prepare(k)
+                if k == 1:
+                    ag_early(1, 1)
 
         at_stage(4, backward)
         at_stage(10, choose(rs_finish, None))

time: 118 us -> 118 us (level)
  no operation moved by 1% of the time
where the time goes in v6:
time: 118 us
  Pallas kernels  118 us (100%)
    pallas_call x1, Pallas kernels, body(): pl.pallas_call(functools.partial(kernel, blocks, factor), out_shape=(pltp...  116 us

profile of v6, /device:TPU:0, one launch (start us, length us, event | category | flops | bytes accessed | tf_op | source)
XLA Modules:
  0.0 118.3 jit_solution(16141588818092503522)
XLA Ops:
  0.6 115.9 %half_step.1 = (bf16[512,1408]{1,0:T(8,128)(2,1)S(1)}, bf16[256,2048]{1,0:T(8,128)(2,1)S(1)}, f32[64,1408]{1,0:T(8,128)S(1)}, f32[64,1408]{1,0:T(8,128)S(1)}, f32[1,2048]{1,0:T(1,128)S(1)}) custom-call(bf16[256,2048]{1,0:T(8,128)(2,1)} %later_hbm.1, bf16[256,2048]{1,0:T(8,128)(2,1)} %earlier_hbm.1, bf16[512,1408]{1,0:T(8,128)(2,1)} %cot_hbm.1, ...), custom_call_target="tpu_custom_call" | custom-call | flops 23622320128 | bytes 16777216 | tf_op jit(solution)/shard_map/half_step/pallas_call | solution.py:578
  116.5 1.7 %hand_over.1 = (bf16[512,1408]{1,0:T(8,128)(2,1)}, bf16[256,2048]{1,0:T(8,128)(2,1)}, f32[64,1408]{1,0:T(8,128)}, f32[64,1408]{1,0:T(8,128)}, f32[1,2048]{1,0:T(1,128)}) custom-call(bf16[512,1408]{1,0:T(8,128)(2,1)S(1)} %get-tuple-element.15.refs_0_, bf16[256,2048]{1,0:T(8,128)(2,1)S(1)} %get-tuple-element.16.refs_1_, ...), custom_call_target="tpu_custom_call" | custom-call | tf_op jit(solution)/shard_map/hand_over/pallas_call | solution.py:556
